TPU v7x, 128 devices: a whole 4x4x4 slice. The times are simulated.
128 devices in a mesh: ep: 32 (over z, y, core), tp: 4 (over x).
Axes of the slice: x: 4, y: 4, z: 4, core: 2. Of those that a mesh axis runs over, the one named last changes fastest.
Arguments:
- value_in: bfloat16 [16384, 2048], P('ep', 'tp'), may hold values from -400 to 400
- gate_in: bfloat16 [16384, 2048], P('ep', 'tp'), may hold values from -8 to 8
- conv_taps: float32 [31, 2048], P(None, 'tp'), may hold values from -1 to 1
- conv_bias: float32 [2048], P('tp'), may hold values from -3 to 3
- ln_gain: float32 [2048], P('tp'), may hold values from 0.1 to 1.9
- ln_bias: float32 [2048], P('tp'), may hold values from -3 to 3
- out_proj: bfloat16 [2048, 4096], P('tp'), may hold values from -0.125 to 0.125
- tokens_b: bfloat16 [16384, 4096], P('ep'), may hold values from -6 to 6
- norm_gain: float32 [4096], replicated, may hold values from 0.1 to 1.9
- routes: int32 [16384, 2], P(('ep', 'tp')), may hold values from 0 to 31, all different within a row; in each aligned block of 128 rows (0 to 127, 128 to 255, ...) at most 12 rows name the same one
- route_weights: float32 [16384, 2], P(('ep', 'tp')), may hold values from 0.2 to 1.5
- expert_gate: bfloat16 [32, 4096, 1024], P('ep', None, 'tp'), may hold values from -0.09375 to 0.09375
- expert_up: bfloat16 [32, 4096, 1024], P('ep', None, 'tp'), may hold values from -0.09375 to 0.09375
- expert_down: bfloat16 [32, 1024, 4096], P('ep', 'tp'), may hold values from -0.1875 to 0.1875
- shared_gate: bfloat16 [4096, 1024], P(None, 'tp'), may hold values from -0.09375 to 0.09375
- shared_up: bfloat16 [4096, 1024], P(None, 'tp'), may hold values from -0.09375 to 0.09375
- shared_down: bfloat16 [1024, 4096], P('tp'), may hold values from -0.1875 to 0.1875
Outputs:
- mixer_out: bfloat16 [16384, 4096], P(('ep', 'tp'))
- experts_out: bfloat16 [16384, 4096], P(('ep', 'tp'))
Inputs may be any that keep to these rules, and one draw needn't show every extreme that they name: `routes`: each row names 2 different experts. In each aligned block of 128 rows (the rows of one device) no expert is named by more than 12 rows, and in some blocks an expert is named by exactly 12 rows.
All inputs are finite; a program needn't handle non-finite values.
Results may differ from a plain program's by a relative error of at most 0.012.
Values may be sent and summed in bfloat16 or wider, within the bound.
No kernel may reach another device: no remote copies, remote signals or barrier semaphores. Data moves between devices by JAX's collectives and lax.ppermute only.
A program may use at most 128 MiB of HBM per device.

v0:
```python
import jax
import jax.numpy as jnp
from jax import lax
from jax.sharding import PartitionSpec as P

EPSILON = 1e-06


def shifted(x, axis, by):
    devices = lax.axis_size(axis)
    pairs = [(i, i + by) for i in range(devices) if 0 <= i + by < devices]
    return lax.ppermute(x, axis, pairs)


def from_everyone(x, axis):
    devices = lax.axis_size(axis)
    return lax.all_to_all(jnp.broadcast_to(x[None], (devices, *x.shape)), axis, 0, 0, tiled=True)


def taken_together(x, axis):
    everything = from_everyone(x, axis)
    return jnp.sum(everything, axis=0)


def packed_total(arrays, axis):
    ends = [0]
    for a in arrays:
        ends.append(ends[-1] + a.size)
    running = taken_together(jnp.concatenate([a.ravel() for a in arrays]), axis)
    return tuple((running[b:e].reshape(a.shape) for a, b, e in zip(arrays, ends, ends[1:])))


def joined_along(blocks, dim):
    blocks = jnp.moveaxis(blocks, 0, dim)
    dims = blocks.shape
    return blocks.reshape(*dims[:dim], dims[dim] * dims[dim + 1], *dims[dim + 2 :])


def gathered_copies(x, axis, dim):
    return joined_along(from_everyone(x, axis), dim)


def slot_table(route_ids, expert_count):
    chosen = route_ids.reshape(-1)
    onehot = (chosen[:, None] == jnp.arange(expert_count, dtype=jnp.int32)[None, :]).astype(
        jnp.int32
    )
    earlier = jnp.cumsum(onehot, axis=0) - onehot
    return (chosen, jnp.sum(earlier * onehot, axis=1))


def gated_hidden(rows_in, weight_gate, weight_up):
    row_shape = rows_in.shape
    matrix = rows_in.reshape(-1, row_shape[-1])
    hidden = (
        jax.nn.silu(jnp.dot(matrix, weight_gate, preferred_element_type=jnp.float32))
        * jnp.dot(matrix, weight_up, preferred_element_type=jnp.float32)
    ).astype(jnp.bfloat16)
    return hidden.reshape(row_shape[:-1] + (weight_gate.shape[1],))


def project_down(hidden, weight):
    row_shape = hidden.shape
    product = jnp.dot(hidden.reshape(-1, row_shape[-1]), weight, preferred_element_type=jnp.float32)
    return product.reshape(row_shape[:-1] + (weight.shape[1],))


def per_device(
    value_in,
    gate_in,
    conv_taps,
    conv_bias,
    ln_gain,
    ln_bias,
    out_proj,
    tokens_b,
    norm_gain,
    routes,
    route_weights,
    expert_gate,
    expert_up,
    expert_down,
    shared_gate,
    shared_up,
    shared_down,
):
    tp_count = lax.axis_size("tp")
    ep_count = lax.axis_size("ep")
    gated = (value_in.astype(jnp.float32) * jax.nn.sigmoid(gate_in.astype(jnp.float32))).astype(
        jnp.bfloat16
    )
    rim_rows = conv_taps.shape[0] - 1
    length = gated.shape[0]
    before = shifted(gated[length - rim_rows :], "ep", 1)
    padded = jnp.concatenate([before, gated], axis=0).astype(jnp.float32)
    filtered = jnp.zeros(gated.shape, jnp.float32) + conv_bias[None, :]
    for tap_index in range(rim_rows + 1):
        filtered = filtered + conv_taps[tap_index][None, :] * padded[tap_index : tap_index + length]
    row_sum, squares = packed_total(
        (jnp.sum(filtered, axis=1), jnp.sum(filtered * filtered, axis=1)), "tp"
    )
    channel_count = filtered.shape[1] * tp_count
    average = row_sum / channel_count
    variance = squares / channel_count - average * average
    normed_a = (filtered - average[:, None]) * lax.rsqrt(
        variance[:, None] + EPSILON
    ) * ln_gain + ln_bias
    activated = jax.nn.silu(normed_a).astype(jnp.bfloat16)
    features = tokens_b.astype(jnp.float32)
    normed_b = (
        features
        * lax.rsqrt(jnp.mean(features * features, axis=1, keepdims=True) + EPSILON)
        * norm_gain
    ).astype(jnp.bfloat16)
    rows_own, top_count = routes.shape
    model_width = normed_b.shape[1]
    own_rows = lax.dynamic_slice_in_dim(normed_b, lax.axis_index("tp") * rows_own, rows_own, 0)
    capacity = max(2, 3 * rows_own * top_count // (2 * ep_count))
    chosen, places = slot_table(routes, ep_count)
    source = jnp.repeat(own_rows, top_count, axis=0)
    outbox = (
        jnp.zeros((ep_count, capacity, model_width), jnp.bfloat16).at[chosen, places].set(source)
    )
    gate_local = expert_gate[0]
    up_local = expert_up[0]
    down_local = expert_down[0]
    arrived = lax.all_to_all(outbox, "ep", split_axis=0, concat_axis=0, tiled=True)
    hidden_routed = gated_hidden(gathered_copies(arrived[None], "tp", 0), gate_local, up_local)
    hidden_routed = hidden_routed.reshape(tp_count, ep_count * capacity, -1)
    hidden_shared = gated_hidden(normed_b, shared_gate, shared_up).reshape(tp_count, rows_own, -1)
    mixer_rows = lax.psum_scatter(
        jnp.dot(activated, out_proj, preferred_element_type=jnp.float32).astype(jnp.bfloat16),
        "tp",
        scatter_dimension=0,
        tiled=True,
    )
    summed = lax.psum_scatter(
        jnp.concatenate(
            [project_down(hidden_routed, down_local), project_down(hidden_shared, shared_down)],
            axis=1,
        ).astype(jnp.bfloat16),
        "tp",
        scatter_dimension=0,
        tiled=True,
    ).astype(jnp.float32)[0]
    summed = summed.astype(jnp.bfloat16)
    routed_rows = summed[: ep_count * capacity].reshape(ep_count, capacity, model_width)
    shared_rows = summed[ep_count * capacity :]
    returned = lax.all_to_all(routed_rows, "ep", split_axis=0, concat_axis=0, tiled=True)
    picked = returned[chosen, places].astype(jnp.float32) * route_weights.reshape(-1)[:, None]
    experts_out = (
        shared_rows.astype(jnp.float32)
        + jnp.sum(picked.reshape(rows_own, top_count, model_width), axis=1)
    ).astype(jnp.bfloat16)
    return (mixer_rows, experts_out)


def solution(mesh):
    return jax.shard_map(
        per_device,
        mesh=mesh,
        in_specs=(
            P("ep", "tp"),
            P("ep", "tp"),
            P(None, "tp"),
            P("tp"),
            P("tp"),
            P("tp"),
            P("tp", None),
            P("ep", None),
            P(),
            P(("ep", "tp"), None),
            P(("ep", "tp"), None),
            P("ep", None, "tp"),
            P("ep", None, "tp"),
            P("ep", "tp", None),
            P(None, "tp"),
            P(None, "tp"),
            P("tp", None),
        ),
        out_specs=(P(("ep", "tp"), None), P(("ep", "tp"), None)),
        check_vma=False,
    )
```

profile of v0, /device:TPU:0, one launch (start us, length us, event | category | flops | bytes accessed | tf_op | source)
XLA Modules:
  0.0 628.7 jit_solution(1816978433081984892)
XLA Ops:
  7.2 0.9 copy.48
  8.1 0.1 eq.29
  8.3 0.1 eq.25
  8.4 0.1 reshape.118
  8.6 0.6 reduce-window.6
  9.2 0.2 slice_reduce_fusion
  9.4 3.1 fusion
  12.5 3.8 fusion.2
  16.4 1.9 copy-done.3
  18.4 3.5 broadcast_in_dim.10
  21.9 4.1 reshape.133
  26.1 2.0 broadcast_in_dim.9
  28.2 66.6 %scatter_fusion = bf16[32,12,4096]{2,0,1:T(8,128)(2,1)} fusion(bf16[32,12,4096]{2,0,1:T(8,128)(2,1)} %broadcast_in_dim.9, s32[256]{0:T(256)S(1)} %bitcast.82, bf16[256,4096]{1,0:T(8,128)(2,1)} %reshape.133), kind=kCustom, calls=%fused_computation.1 | custom fusion | bytes 6293504 | tf_op jit(solution)/shard_map/scatter | solution.py:122
  94.8 3.7 copy.52
  98.5 59.3 %all_to_all.21 = bf16[32,12,4096]{2,1,0:T(8,128)(2,1)S(1)} all-to-all(bf16[32,12,4096]{2,1,0:T(8,128)(2,1)S(1)} %copy.52), channel_id=1, replica_groups=mesh['ep'=32,'tp'=4] {'ep'}, dimensions={0} | all-to-all | bytes 6291456 | tf_op jit(solution)/shard_map/all_to_all | solution.py:127
  157.8 3.4 copy.53
  161.2 8.1 %broadcast_in_dim.11 = bf16[4,1,32,12,4096]{4,2,3,1,0:T(8,128)(2,1)} broadcast(bf16[32,12,4096]{2,0,1:T(8,128)(2,1)} %copy.53), dimensions={2,3,4} | broadcast | bytes 15728640 | tf_op jit(solution)/shard_map/broadcast_in_dim | solution.py:17
  169.2 6.7 %all-to-all-start.2 = ((bf16[4,1,32,12,4096]{4,2,3,1,0:T(8,128)(2,1)}), bf16[4,1,32,12,4096]{4,2,3,1,0:T(8,128)(2,1)}, u32[]{:S(2)}, u32[]{:S(2)}) async-start(bf16[4,1,32,12,4096]{4,2,3,1,0:T(8,128)(2,1)} %broadcast_in_dim.11), calls=%async_computation.3 | async-start | bytes 25165824 | tf_op jit(solution)/shard_map/all_to_all | solution.py:17
  176.0 4.1 fusion.64
  180.1 9.9 %convolution_convert_fusion.1 = bf16[512,4096]{1,0:T(8,128)(2,1)} fusion(bf16[256,4096]{1,0:T(8,128)(2,1)} %param.33, bf16[512,4096]{1,0:T(8,128)(2,1)} %copy-done.3, bf16[4096,256]{1,0:T(8,128)(2,1)} %param.32, f32[512,256]{1,0:T(8,128)S(1)} %fusion.64), kind=kOutput, calls=%fused_computation.9 | convolution fusion | flops 2150367232 | bytes 13107200 | tf_op jit(solution)/shard_map/dot_general | solution.py:64
  190.0 125.3 %all-to-all-done.2 = bf16[4,1,32,12,4096]{4,2,3,1,0:T(8,128)(2,1)} async-done(((bf16[4,1,32,12,4096]{4,2,3,1,0:T(8,128)(2,1)}), bf16[4,1,32,12,4096]{4,2,3,1,0:T(8,128)(2,1)}, u32[]{:S(2)}, u32[]{:S(2)}) %all-to-all-start.2) | async-done | bytes 12582944 | tf_op jit(solution)/shard_map/all_to_all | solution.py:17
  315.2 13.8 %copy.54 = bf16[4,1,32,12,4096]{4,3,2,0,1:T(8,128)(2,1)} copy(bf16[4,1,32,12,4096]{4,2,3,1,0:T(8,128)(2,1)} %all-to-all-done.2) | data formatting | bytes 25165824 | tf_op jit(solution)/shard_map/all_to_all | solution.py:17
  329.0 18.2 %reshape_reshape.3 = bf16[1536,4096]{1,0:T(8,128)(2,1)} reshape(bf16[4,1,32,12,4096]{4,3,2,0,1:T(8,128)(2,1)} %copy.54) | data formatting | bytes 25165824 | tf_op jit(solution)/shard_map/reshape;reshape | solution.py:54
  347.2 7.7 %fusion.7 = f32[1536,256]{1,0:T(8,128)S(1)} fusion(bf16[1536,4096]{1,0:T(8,128)(2,1)} %reshape_reshape.3, bf16[1,4096,256]{2,1,0:T(8,128)(2,1)} %param.28), kind=kOutput, calls=%fused_computation.18 | convolution fusion | flops 3221225472 | bytes 16252928 | tf_op jit(solution)/shard_map/dot_general | solution.py:56
  354.9 1.0 copy-done.2
  356.0 0.6 copy-done.12
  356.6 3.9 fusion.3
  360.5 6.4 %convolution_convert_fusion = bf16[4,384,4096]{2,1,0:T(8,128)(2,1)} fusion(bf16[4,384,256]{2,1,0:T(8,128)(2,1)S(1)} %bitcast.84, bf16[1,256,4096]{2,1,0:T(8,128)(2,1)S(1)} %copy-done), kind=kOutput, calls=%fused_computation.5 | convolution fusion | flops 3227516928 | bytes 15466496 | tf_op jit(solution)/shard_map/dot_general | solution.py:64
  366.9 12.3 %pad_maximum_fusion = bf16[4,512,4096]{2,1,0:T(8,128)(2,1)} fusion(bf16[4,128,4096]{2,1,0:T(8,128)(2,1)S(1)} %bitcast.83, bf16[4,384,4096]{2,1,0:T(8,128)(2,1)} %convolution_convert_fusion), kind=kLoop, calls=%fused_computation.2 | loop fusion | flops 33554432 | bytes 33554432 | tf_op jit(solution)/shard_map/concatenate | solution.py:138
  379.3 0.9 copy-done.5
  380.3 0.2 copy-done.6
  380.4 0.3 multiply_convert_fusion.1
  380.8 1.3 collective-permute-start
  382.1 0.8 collective-permute-done
  382.9 0.2 maximum_convert_fusion
  383.1 5.0 fusion.59
  388.1 8.2 %all_to_all.22 = f32[4,1,1024]{2,1,0:T(1,128)S(1)} all-to-all(f32[4,1,1024]{2,1,0:T(1,128)S(1)} %broadcast_in_dim.8), channel_id=1, replica_groups=mesh['ep'=32,'tp'=4] {'tp'}, dimensions={0} | all-to-all | bytes 32768 | tf_op jit(solution)/shard_map/all_to_all | solution.py:17
  396.4 6.8 %convolution_convert_fusion.2 = bf16[512,4096]{1,0:T(8,128)(2,1)} fusion(bf16[512,4096]{1,0:T(8,128)(2,1)} %param.23, f32[512,512]{1,0:T(8,128)S(1)} %get-tuple-element.6, f32[512]{0:T(512)S(1)} %copy-done.13, f32[512]{0:T(512)S(1)} %copy-done.14, f32[512]{0:T(512)S(1)} %get-tuple-element.39, f32[512]{0:T(512)S(1)} %get-tuple-element.38), kind=kOutput, calls=%fused_computation.10 | convolution fusion | flops 2151940096 | bytes 9445376 | tf_op jit(solution)/shard_map/dot_general | solution.py:132
  403.2 120.4 %reduce-scatter.5.cloned.1.call-done = bf16[1,512,4096]{2,1,0:T(8,128)(2,1)} async-done(((bf16[4,512,4096]{2,1,0:T(8,128)(2,1)}), bf16[1,512,4096]{2,1,0:T(8,128)(2,1)}) %reduce-scatter.5.cloned.1.call-update) | async-done | bytes 4194320 | tf_op jit(solution)/shard_map/reduce_scatter | solution.py:137
  523.6 3.9 slice.316
  527.5 5.5 reshape.122
  533.0 7.5 %all-to-all-start.3 = ((bf16[32,12,4096]{2,1,0:T(8,128)(2,1)}), bf16[32,12,4096]{2,1,0:T(8,128)(2,1)}, u32[]{:S(2)}, u32[]{:S(2)}) async-start(bf16[32,12,4096]{2,1,0:T(8,128)(2,1)} %reshape.122), calls=%async_computation.5 | async-start | bytes 8388608 | tf_op jit(solution)/shard_map/all_to_all | solution.py:149
  540.6 53.8 %all-to-all-done.3 = bf16[32,12,4096]{2,1,0:T(8,128)(2,1)} async-done(((bf16[32,12,4096]{2,1,0:T(8,128)(2,1)}), bf16[32,12,4096]{2,1,0:T(8,128)(2,1)}, u32[]{:S(2)}, u32[]{:S(2)}) %all-to-all-start.3) | async-done | bytes 3145760 | tf_op jit(solution)/shard_map/all_to_all | solution.py:149
  594.5 5.6 copy.55
  600.1 6.0 gather_fusion
  606.1 4.2 reshape.124
  610.3 8.9 %multiply_reduce_fusion = f32[128,4096]{1,0:T(8,128)S(1)} fusion(f32[128,2,4096]{2,1,0:T(2,128)} %reshape.124, f32[128,2]{1,0:T(8,128)S(1)} %copy.56), kind=kLoop, calls=%fused_computation.11 | loop fusion | flops 1572864 | bytes 6292480 | tf_op jit(solution)/shard_map/reduce_sum | solution.py:153
  619.1 2.4 fusion.4
  (46 shorter events, 0.7 us)
Async XLA Ops:
  7.2 353.3 %copy-start = (bf16[1,256,4096]{2,1,0:T(8,128)(2,1)S(1)}, bf16[1,256,4096]{2,1,0:T(8,128)(2,1)}, u32[]{:S(2)}) copy-start(bf16[1,256,4096]{2,1,0:T(8,128)(2,1)} %param.30) | copy-start | bytes 6291460
  7.2 5.3 copy-start.8
  9.4 6.9 %copy-start.9 = (s32[32,3]{0,1:T(4,128)}, s32[32,3]{0,1:T(4,128)S(1)}, u32[]{:S(2)}) copy-start(s32[32,3]{0,1:T(4,128)S(1)} %reduce-window.9) | copy-start | bytes 1156
  16.3 2.0 copy-start.3
  18.4 7.6 %slice-start = ((s32[32,3]{0,1:T(4,128)}), s32[32,2]{0,1:T(2,128)S(1)}, s32[]{:S(2)}) async-start(s32[32,3]{0,1:T(4,128)} %copy-done.9), calls=%async_computation.8 | async-start | bytes 2048 | tf_op jit(solution)/shard_map/slice.1
  169.2 146.0 %all-to-all-start.2 = ((bf16[4,1,32,12,4096]{4,2,3,1,0:T(8,128)(2,1)}), bf16[4,1,32,12,4096]{4,2,3,1,0:T(8,128)(2,1)}, u32[]{:S(2)}, u32[]{:S(2)}) async-start(bf16[4,1,32,12,4096]{4,2,3,1,0:T(8,128)(2,1)} %broadcast_in_dim.11), calls=%async_computation.3 | async-start | bytes 25165824 | tf_op jit(solution)/shard_map/all_to_all | solution.py:17
  175.9 347.7 %reduce-scatter.5.cloned.1.call-start = ((), (), s32[]{:S(2)}) async-start(), calls=%async_computation.7 | async-start | bytes 20971520 | tf_op jit(solution)/shard_map/reduce_scatter | solution.py:137
  347.2 8.8 %copy-start.2 = (bf16[1536,4096]{1,0:T(8,128)(2,1)S(1)}, bf16[1536,4096]{1,0:T(8,128)(2,1)}, u32[]{:S(2)}) copy-start(bf16[1536,4096]{1,0:T(8,128)(2,1)} %reshape_reshape.3) | copy-start | bytes 37748740
  347.2 9.4 %copy-start.12 = (bf16[1,4096,256]{2,1,0:T(8,128)(2,1)S(1)}, bf16[1,4096,256]{2,1,0:T(8,128)(2,1)}, u32[]{:S(2)}) copy-start(bf16[1,4096,256]{2,1,0:T(8,128)(2,1)} %param.29) | copy-start | bytes 6291460
  360.5 6.4 %copy-start.4 = (bf16[512,4096]{1,0:T(8,128)(2,1)S(1)}, bf16[512,4096]{1,0:T(8,128)(2,1)}, u32[]{:S(2)}) copy-start(bf16[512,4096]{1,0:T(8,128)(2,1)} %convolution_convert_fusion.1) | copy-start | bytes 12582916
  379.2 1.0 copy-start.5
  379.2 1.2 copy-start.6
  379.3 2.8 copy-start.7
  379.3 3.8 copy-start.10
  379.3 242.3 %reduce-scatter.3.cloned.1.call-start = ((), (), s32[]{:S(2)}) async-start(), calls=%async_computation.6 | async-start | bytes 5242880 | tf_op jit(solution)/shard_map/reduce_scatter | solution.py:131
  380.8 2.1 collective-permute-start
  383.1 13.3 %copy-start.13 = (f32[512]{0:T(512)S(1)}, f32[512]{0:T(512)}, u32[]{:S(2)}) copy-start(f32[512]{0:T(512)} %param.22) | copy-start | bytes 6148
  383.1 13.3 %copy-start.14 = (f32[512]{0:T(512)S(1)}, f32[512]{0:T(512)}, u32[]{:S(2)}) copy-start(f32[512]{0:T(512)} %param.21) | copy-start | bytes 6148
  533.0 7.5 %copy-start.11 = (f32[128,2]{0,1:T(2,128)S(1)}, f32[128,2]{0,1:T(2,128)}, u32[]{:S(2)}) copy-start(f32[128,2]{0,1:T(2,128)} %param.27) | copy-start | bytes 3076
  533.0 61.5 %all-to-all-start.3 = ((bf16[32,12,4096]{2,1,0:T(8,128)(2,1)}), bf16[32,12,4096]{2,1,0:T(8,128)(2,1)}, u32[]{:S(2)}, u32[]{:S(2)}) async-start(bf16[32,12,4096]{2,1,0:T(8,128)(2,1)} %reshape.122), calls=%async_computation.5 | async-start | bytes 8388608 | tf_op jit(solution)/shard_map/all_to_all | solution.py:149
  610.3 11.3 %copy-start.1 = (bf16[1,256,4096]{2,1,0:T(8,128)(2,1)S(1)}, bf16[1,256,4096]{2,1,0:T(8,128)(2,1)}, u32[]{:S(2)}) copy-start(bf16[1,256,4096]{2,1,0:T(8,128)(2,1)} %param.30) | copy-start | bytes 6291460
Sparse Core Ops, SparseCore 0:
  379.4 144.1 reduce-scatter.4
  526.6 46.5 reduce-scatter.2
where the time goes:
time: 639 us; the launch traced here: 629 us
  waiting for transfers between devices  300 us (47%)
  local copies, waits for them, and re-layouts  155 us (24%)
  blocking collectives  67.5 us (11%)
  matrix products  38.9 us (6%)
  other arithmetic  36.8 us (6%)
  starting transfers between devices  15.6 us (2%)
  between operations  14.6 us (2%)
    all_to_all x1, waiting for transfers between devices, from_everyone(): lax.all_to_all(jnp.broadcast_to(x[None], (devices, *x.shape)), axis, 0, 0...  125 us
    reduce_scatter x1, waiting for transfers between devices, per_device(): lax.psum_scatter(jnp.concatenate([project_down(hidden_routed, down_local)...  120 us
    scatter x2, local copies, waits for them, and re-layouts, per_device(): jnp.zeros((ep_count, capacity, model_width), jnp.bfloat16)  70.3 us
    all_to_all x1, blocking collectives, per_device(): lax.all_to_all(outbox, 'ep', split_axis=0, concat_axis=0, tiled=True)  59.3 us
    all_to_all x1, waiting for transfers between devices, per_device(): lax.all_to_all(routed_rows, 'ep', split_axis=0, concat_axis=0, tiled=True)  53.8 us
    another operation x1, local copies, waits for them, and re-layouts, gated_hidden(): matrix = rows_in.reshape(-1, row_shape[-1])  18.2 us
    dot_general x2, matrix products, project_down(): jnp.dot(hidden.reshape(-1, row_shape[-1]), weight, preferred_element_type...  16.3 us
    all_to_all x1, local copies, waits for them, and re-layouts, from_everyone(): lax.all_to_all(jnp.broadcast_to(x[None], (devices, *x.shape)), axis, 0, 0...  13.8 us
  transfers between devices with their start and end apart: 5, of which 4 were waited for; matrix products, arithmetic and copies ran while one was open for 10% of the time, Pallas kernels for 0%

commit v1 on v0

v1 whole, which is shorter than its diff:
```python
from functools import partial

import jax
import jax.numpy as jnp
from jax import lax
from jax.experimental import pallas as pl
from jax.experimental.pallas import tpu as pltpu
from jax.sharding import PartitionSpec as P


EPSILON = 1e-06
BF16, F32 = jnp.bfloat16, jnp.float32


def shifted(x, axis, by):
    devices = lax.axis_size(axis)
    pairs = [(i, i + by) for i in range(devices) if 0 <= i + by < devices]
    return lax.ppermute(x, axis, pairs)


def swapped(x, axis, bits):
    return lax.ppermute(x, axis, [(i, i ^ bits) for i in range(lax.axis_size(axis))])


def dot(a, b):
    return jnp.dot(a, b, preferred_element_type=F32)


def dot_rows(a, b):
    return lax.dot_general(a, b, (((1,), (1,)), ((), ())), preferred_element_type=F32)


def gated_product(gate, up):
    return (jax.nn.silu(gate) * up).astype(BF16)


def iota(shape, dim):
    return lax.broadcasted_iota(jnp.int32, shape, dim)


def ones_where(mask):
    return jnp.where(mask, 1.0, 0.0).astype(BF16)


def quotient(x, by):
    return (x * (65536 // by + 1)) >> 16


def places(routes, experts):
    rows = routes.shape[0]
    expert = iota((rows, experts), 1)
    named = (routes[:, 0:1] == expert) | (routes[:, 1:2] == expert)
    earlier = ones_where(iota((rows, rows), 1) < iota((rows, rows), 0))
    return jnp.where(named, dot(earlier, ones_where(named)), -1.0)


def outbox_body(flags, tokens, gain, own, other, out, rows, place, select, *, capacity, chunk):
    step = pl.program_id(0)
    block, width = own.shape[0], gain.shape[1]
    experts = place.shape[1]

    @pl.when(step == 0)
    def _():
        def norm(i, carry):
            at = pl.multiple_of((i % (block // chunk)) * chunk, chunk)
            x = tokens[i // (block // chunk), 0, pl.ds(at, chunk), :].astype(F32)
            scale = lax.rsqrt(jnp.sum(x * x, axis=1, keepdims=True) * (1.0 / width) + EPSILON)
            rows[pl.ds(pl.multiple_of(i * chunk, chunk), chunk), :] = (x * scale * gain[...]).astype(BF16)
            return carry

        lax.fori_loop(0, 2 * block // chunk, norm, 0)
        first = flags[1] == 0
        place[:block, :] = places(jnp.where(first, own[...], other[...]), experts).astype(BF16)
        place[block:, :] = places(jnp.where(first, other[...], own[...]), experts).astype(BF16)
        slots = select.shape[0]
        slot = iota((slots, 1), 0)
        expert = quotient(slot, 2 * capacity)
        within = slot - expert * (2 * capacity)
        second = jnp.where(within >= capacity, 1, 0)
        wanted = (within - second * capacity).astype(F32)
        there = dot_rows(ones_where(expert == iota((slots, experts), 1)), place[...])
        row_block = jnp.where(iota((slots, 2 * block), 1) >= block, 1, 0)
        select[...] = ones_where((there == wanted) & (row_block == second))

    here = out.shape[1]
    at = pl.multiple_of(step * here, here)
    out[...] = dot(select[...], rows[:, pl.ds(at, here)]).astype(BF16)


def outbox_of(flags, tokens, gain, own, other, experts, capacity):
    width = tokens.shape[1]
    block = own.shape[0]
    slots = experts * 2 * capacity
    here = 512
    return pl.pallas_call(
        partial(outbox_body, capacity=capacity, chunk=16),
        grid_spec=pltpu.PrefetchScalarGridSpec(
            num_scalar_prefetch=1,
            grid=(width // here,),
            in_specs=[
                pl.BlockSpec((2, 1, block, width), lambda i, f: (0, f[0], 0, 0)),
                pl.BlockSpec((1, width), lambda i, f: (0, 0)),
                pl.BlockSpec(own.shape, lambda i, f: (0, 0)),
                pl.BlockSpec(other.shape, lambda i, f: (0, 0)),
            ],
            out_specs=pl.BlockSpec((slots, here), lambda i, f: (0, i)),
            scratch_shapes=[
                pltpu.VMEM((2 * block, width), BF16),
                pltpu.VMEM((2 * block, experts), BF16),
                pltpu.VMEM((slots, 2 * block), BF16),
            ],
        ),
        out_shape=jax.ShapeDtypeStruct((slots, width), BF16),
        cost_estimate=pl.CostEstimate(flops=2 * slots * 2 * block * width, bytes_accessed=2 * width * (slots + 2 * block), transcendentals=0),
        name="outbox",
    )(flags, tokens.reshape(2, 2, block, width), gain.reshape(1, width), own, other)


def hidden_body(flags, arrived, gate, up, first, second, kept, sent, sums, hidden, *, capacity, chunk):
    step = pl.program_id(0)
    a = arrived[...]
    weights = (gate, up, first, second)

    @pl.when(step == 0)
    def _():
        for i, w in enumerate(weights):
            sums[i] = dot(a, w[...])

    @pl.when(step != 0)
    def _():
        for i, w in enumerate(weights):
            sums[i] += dot(a, w[...])

    @pl.when(step == pl.num_programs(0) - 1)
    def _():
        units = gate.shape[1]
        half = units // 2

        def activate(i, carry):
            at = pl.ds(pl.multiple_of(i * chunk, chunk), chunk)
            hidden[at, :units] = gated_product(sums[0, at, :], sums[1, at, :])
            hidden[at, units : units + half] = gated_product(sums[2, at, :half], sums[2, at, half:])
            hidden[at, units + half :] = gated_product(sums[3, at, :half], sums[3, at, half:])
            return carry

        lax.fori_loop(0, a.shape[0] // chunk, activate, 0)
        shape = (kept.shape[0], a.shape[0])
        row = iota((shape[0], 1), 0)
        source = row + capacity * quotient(row, capacity)
        lane = iota(shape, 1)
        kept[...] = dot(ones_where(lane == source + capacity * flags[1]), hidden[...]).astype(BF16)
        sent[...] = dot(ones_where(lane == source + capacity * (1 - flags[1])), hidden[...]).astype(BF16)


def hidden_of(flags, arrived, gate, up, first, second, capacity):
    rows, width = arrived.shape
    units = gate.shape[1]
    step = 512
    out = jax.ShapeDtypeStruct((rows // 2, 2 * units), BF16)
    weight = pl.BlockSpec((step, units), lambda k, f: (k, 0))
    whole = pl.BlockSpec(out.shape, lambda k, f: (0, 0))
    return pl.pallas_call(
        partial(hidden_body, capacity=capacity, chunk=64),
        grid_spec=pltpu.PrefetchScalarGridSpec(
            num_scalar_prefetch=1,
            grid=(width // step,),
            in_specs=[pl.BlockSpec((rows, step), lambda k, f: (0, k))] + [weight] * 4,
            out_specs=[whole, whole],
            scratch_shapes=[pltpu.VMEM((4, rows, units), F32), pltpu.VMEM((rows, 2 * units), BF16)],
        ),
        out_shape=[out, out],
        cost_estimate=pl.CostEstimate(flops=8 * rows * width * units, bytes_accessed=2 * width * (rows + 4 * units), transcendentals=0),
        name="hidden",
    )(flags, arrived, gate, up, first, second)


def down_body(flags, kept, got, left, right, out, whole, wide, *, capacity):
    units = whole.shape[1] // 4
    half = units // 2

    @pl.when(pl.program_id(0) == 0)
    def _():
        k, g = kept[...], got[...]
        by_distance = [
            k[:, :units],
            jnp.concatenate([k[:, units : units + half], g[:, units + half :]], axis=1),
            g[:, :units],
            jnp.concatenate([g[:, units : units + half], k[:, units + half :]], axis=1),
        ]
        odd, high = flags[0] == 1, flags[1] == 1
        turned = [jnp.where(odd, by_distance[i ^ 1], by_distance[i]) for i in range(4)]
        for i in range(4):
            whole[:, i * units : (i + 1) * units] = jnp.where(high, turned[i ^ 2], turned[i])

    for side, weight in enumerate((left, right)):
        rows = dot(whole[...], weight[...])
        for expert in range(rows.shape[0] // capacity):
            at = (2 * expert + side) * capacity
            wide[at : at + capacity, :] = rows[expert * capacity : (expert + 1) * capacity, :]
    out[...] = wide[...].astype(BF16)


def down_of(flags, kept, got, down, capacity):
    rows, units = kept.shape[0], down.shape[0]
    width = down.shape[1] // 2
    step = 256
    count = width // step
    whole = pl.BlockSpec(kept.shape, lambda n, f: (0, 0))
    return pl.pallas_call(
        partial(down_body, capacity=capacity),
        grid_spec=pltpu.PrefetchScalarGridSpec(
            num_scalar_prefetch=1,
            grid=(count,),
            in_specs=[
                whole,
                whole,
                pl.BlockSpec((units, step), lambda n, f: (0, n)),
                pl.BlockSpec((units, step), lambda n, f: (0, n + count)),
            ],
            out_specs=pl.BlockSpec((2 * rows, step), lambda n, f: (0, n)),
            scratch_shapes=[pltpu.VMEM((rows, units), BF16), pltpu.VMEM((2 * rows, step), F32)],
        ),
        out_shape=jax.ShapeDtypeStruct((2 * rows, width), BF16),
        cost_estimate=pl.CostEstimate(flops=4 * rows * units * width, bytes_accessed=4 * width * (rows + units), transcendentals=0),
        name="down",
    )(flags, kept, got, down, down)


def product_body(a, b, out):
    out[...] = dot(a[...], b[...]).astype(BF16)


def product_of(a, b):
    rows, width = a.shape[0], b.shape[1]
    block = 128
    return pl.pallas_call(
        product_body,
        grid=(rows // block,),
        in_specs=[pl.BlockSpec((block, a.shape[1]), lambda i: (i, 0)), pl.BlockSpec(b.shape, lambda i: (0, 0))],
        out_specs=pl.BlockSpec((block, width), lambda i: (i, 0)),
        out_shape=jax.ShapeDtypeStruct((rows, width), BF16),
        cost_estimate=pl.CostEstimate(flops=2 * rows * width * b.shape[0], bytes_accessed=2 * width * (rows + b.shape[0]), transcendentals=0),
    )(a, b)


def shared_body(flags, hidden, down, send_1, keep_1, send_3, keep_3):
    me = flags[0] + 2 * flags[1]
    block, width = send_1.shape[0] // 2, send_1.shape[1]
    targets = (
        ((keep_1, 0), (keep_3, 0)),
        ((send_1, 0), (keep_3, 1)),
        ((send_1, 1), (send_3, 1)),
        ((keep_1, 1), (send_3, 0)),
    )
    for away, sides in enumerate(targets):
        at = pl.multiple_of((me ^ away) * block, block)
        for side, (out, place) in enumerate(sides):
            product = dot(hidden[pl.ds(at, block), :], down[:, side * width : (side + 1) * width])
            out[place * block : (place + 1) * block, :] = product.astype(BF16)


def shared_parts_of(flags, hidden, down):
    rows, width = hidden.shape[0], down.shape[1]
    out = jax.ShapeDtypeStruct((rows // 2, width // 2), BF16)
    whole = pl.BlockSpec(out.shape, lambda i, f: (0, 0))
    return pl.pallas_call(
        shared_body,
        grid_spec=pltpu.PrefetchScalarGridSpec(
            num_scalar_prefetch=1,
            grid=(1,),
            in_specs=[pl.BlockSpec(hidden.shape, lambda i, f: (0, 0)), pl.BlockSpec(down.shape, lambda i, f: (0, 0))],
            out_specs=[whole] * 4,
        ),
        out_shape=[out] * 4,
        cost_estimate=pl.CostEstimate(flops=2 * rows * width * down.shape[0], bytes_accessed=2 * width * (rows + down.shape[0]), transcendentals=0),
        name="shared_product",
    )(flags, hidden, down)


def portions_body(routes, weights, mix, *, capacity, experts):
    block, slots = routes.shape[0], mix.shape[2]
    chosen = routes[...]
    expert = iota((block, experts), 1)
    weight = jnp.where(chosen[:, 0:1] == expert, weights[:, 0:1], 0.0) + jnp.where(
        chosen[:, 1:2] == expert, weights[:, 1:2], 0.0
    )
    upper = weight.astype(BF16)
    lower = (weight - upper.astype(F32)).astype(BF16)
    lane = iota((experts, slots), 1)
    unfold = ones_where(quotient(lane, 2 * capacity) == iota((experts, slots), 0))
    lane = iota((1, slots), 1)
    within = lane - quotient(lane, 2 * capacity) * (2 * capacity)
    second = jnp.where(within >= capacity, 1, 0)
    wanted = (within - second * capacity).astype(F32)
    hit = dot(places(chosen, experts).astype(BF16), unfold) == wanted
    for part, values in enumerate((upper, lower)):
        there = dot(values, unfold)
        for side in range(2):
            mix[side, part * block : (part + 1) * block, :] = jnp.where(
                hit & (second == side), there, 0.0
            ).astype(BF16)


def portions_of(routes, weights, experts, capacity):
    block, slots = routes.shape[0], 2 * experts * capacity
    return pl.pallas_call(
        partial(portions_body, capacity=capacity, experts=experts),
        out_shape=jax.ShapeDtypeStruct((2, 2 * block, slots), BF16),
        cost_estimate=pl.CostEstimate(flops=6 * block * slots * experts, bytes_accessed=8 * block * slots, transcendentals=0),
        name="portions",
    )(routes, weights)


def mix_body(portions, returned, shared, out):
    block = out.shape[0]
    both = dot(portions[pl.program_id(1)], returned[...])
    out[...] = (shared[...].astype(F32) + (both[:block] + both[block:])).astype(BF16)


def mixed_of(portions, returned, shared):
    slots, width = returned.shape
    block = shared.shape[0]
    step = 512
    count = width // step
    return pl.pallas_call(
        mix_body,
        grid=(count, 2),
        in_specs=[
            pl.BlockSpec(portions.shape, lambda n, h: (0, 0, 0)),
            pl.BlockSpec((slots, step), lambda n, h: (0, n)),
            pl.BlockSpec((block, step), lambda n, h: (0, h * count + n)),
        ],
        out_specs=pl.BlockSpec((block, step), lambda n, h: (0, h * count + n)),
        out_shape=jax.ShapeDtypeStruct((block, 2 * width), BF16),
        cost_estimate=pl.CostEstimate(flops=8 * block * slots * width, bytes_accessed=2 * width * (slots + 4 * block), transcendentals=0),
        name="mix",
    )(portions, returned, shared)


def gated_of(value_in, gate_in):
    return (value_in.astype(F32) * jax.nn.sigmoid(gate_in.astype(F32))).astype(BF16)


def convolved(before, gated, conv_taps, conv_bias):
    length = gated.shape[0]
    padded = jnp.concatenate([before, gated], axis=0).astype(F32)
    filtered = jnp.zeros(gated.shape, F32) + conv_bias[None, :]
    for tap_index in range(conv_taps.shape[0]):
        filtered = filtered + conv_taps[tap_index][None, :] * padded[tap_index : tap_index + length]
    return filtered


def per_device(
    value_in,
    gate_in,
    conv_taps,
    conv_bias,
    ln_gain,
    ln_bias,
    out_proj,
    tokens_b,
    norm_gain,
    routes,
    route_weights,
    expert_gate,
    expert_up,
    expert_down,
    shared_gate,
    shared_up,
    shared_down,
):
    tp_count = lax.axis_size("tp")
    ep_count = lax.axis_size("ep")
    me = lax.axis_index("tp")
    flags = jnp.stack([me & 1, me >> 1]).astype(jnp.int32)
    rows_own, top_count = routes.shape
    capacity = max(2, 3 * rows_own * top_count // (2 * ep_count))
    width = tokens_b.shape[1]
    gate_local, up_local, down_local = expert_gate[0], expert_up[0], expert_down[0]
    half = gate_local.shape[1] // 2
    down_all = lax.all_gather(down_local, "tp", axis=0, tiled=True)

    other_routes = swapped(routes, "tp", 2)

    rim = value_in.shape[0] - (conv_taps.shape[0] - 1)
    tail = gated_of(value_in[rim:], gate_in[rim:])
    before = shifted(tail, "ep", 1)

    first = jnp.concatenate([gate_local[:, :half], up_local[:, :half]], axis=1)
    second = jnp.concatenate([gate_local[:, half:], up_local[:, half:]], axis=1)
    first_of_1 = swapped(first, "tp", 1)
    second_of_3 = swapped(second, "tp", 3)

    outbox = outbox_of(flags, tokens_b, norm_gain, routes, other_routes, ep_count, capacity)
    arrived = lax.all_to_all(
        outbox.reshape(ep_count, 2 * capacity, width), "ep", split_axis=0, concat_axis=0, tiled=True
    ).reshape(2 * capacity * ep_count, width)
    tokens_b, value_in, gate_in, outbox = lax.optimization_barrier((tokens_b, value_in, gate_in, outbox))

    filtered = convolved(before, gated_of(value_in, gate_in), conv_taps, conv_bias)
    sums = jnp.stack([jnp.sum(filtered, axis=1), jnp.sum(filtered * filtered, axis=1)])
    other_sums = [swapped(sums, "tp", bits) for bits in (1, 2, 3)]

    features = tokens_b.astype(F32)
    normed_b = (
        features
        * lax.rsqrt(jnp.mean(features * features, axis=1, keepdims=True) + EPSILON)
        * norm_gain
    ).astype(BF16)
    hidden_shared = gated_product(dot(normed_b, shared_gate), dot(normed_b, shared_up))
    send_1, keep_1, send_3, keep_3 = shared_parts_of(flags, hidden_shared, shared_down)

    *other_sums, hidden_shared, send_1, send_3 = lax.optimization_barrier(
        (*other_sums, hidden_shared, send_1, send_3)
    )
    total = sums + other_sums[0] + (other_sums[1] + other_sums[2])
    channel_count = filtered.shape[1] * tp_count
    average = total[0] / channel_count
    variance = total[1] / channel_count - average * average
    normed_a = (filtered - average[:, None]) * lax.rsqrt(
        variance[:, None] + EPSILON
    ) * ln_gain + ln_bias
    activated = jax.nn.silu(normed_a).astype(BF16)
    mixer_parts = product_of(activated, out_proj)
    mixer_rows = lax.psum_scatter(mixer_parts, "tp", scatter_dimension=0, tiled=True)

    kept, sent = hidden_of(flags, arrived, gate_local, up_local, first_of_1, second_of_3, capacity)
    got = swapped(sent, "tp", 2)

    left_1 = swapped(send_1, "tp", 1)
    right_1 = swapped(send_3, "tp", 3)

    expert_rows = down_of(flags, kept, got, down_all, capacity)
    returned = lax.all_to_all(
        expert_rows.reshape(ep_count, 2 * capacity, width // 2), "ep", split_axis=0, concat_axis=0, tiled=True
    ).reshape(2 * capacity * ep_count, width // 2)
    left_sum = keep_1.astype(F32) + left_1.astype(F32)
    right_sum = keep_3.astype(F32) + right_1.astype(F32)
    left_on, right_on = left_sum[rows_own:].astype(BF16), right_sum[rows_own:].astype(BF16)
    left_2 = swapped(left_on, "tp", 3)
    right_2 = swapped(right_on, "tp", 1)
    shared_rows = jnp.concatenate(
        [left_sum[:rows_own] + left_2.astype(F32), right_sum[:rows_own] + right_2.astype(F32)], axis=1
    ).astype(BF16)
    portions = portions_of(routes, route_weights, ep_count, capacity)
    experts_out = mixed_of(portions, returned, shared_rows)
    return (mixer_rows, experts_out)


def solution(mesh):
    return jax.shard_map(
        per_device,
        mesh=mesh,
        in_specs=(
            P("ep", "tp"),
            P("ep", "tp"),
            P(None, "tp"),
            P("tp"),
            P("tp"),
            P("tp"),
            P("tp", None),
            P("ep", None),
            P(),
            P(("ep", "tp"), None),
            P(("ep", "tp"), None),
            P("ep", None, "tp"),
            P("ep", None, "tp"),
            P("ep", "tp", None),
            P(None, "tp"),
            P(None, "tp"),
            P("tp", None),
        ),
        out_specs=(P(("ep", "tp"), None), P(("ep", "tp"), None)),
        check_vma=False,
    )
```

time: 639 us -> 260 us (0.41); the launches traced: 629 us -> 259 us
  waiting for transfers between devices: 300 us -> 121 us
  local copies, waits for them, and re-layouts: 155 us -> 10.7 us
  blocking collectives: 67.5 us -> 0 us
  Pallas kernels: 0 us -> 58 us
  matrix products: 38.9 us -> 3.33 us
  other arithmetic: 36.8 us -> 17.6 us
  starting transfers between devices: 15.6 us -> 34.1 us
    all_to_all x2, waiting for transfers between devices: 179 us -> 15.3 us  [the longest x1 15.3 us: per_device(): lax.all_to_all(expert_rows.reshape(ep_count, 2 * capacity, width // 2), '...]
    reduce_scatter x2 -> x1, waiting for transfers between devices: 120 us -> 0.01 us  [per_device(): lax.psum_scatter(mixer_parts, 'tp', scatter_dimension=0, tiled=True)]
    ppermute x0 -> x11, waiting for transfers between devices: none -> 105 us  [swapped(): lax.ppermute(x, axis, [(i, i ^ bits) for i in range(lax.axis_size(axis))])]
    scatter x2 -> x0, local copies, waits for them, and re-layouts: 70.3 us -> none  [per_device(): jnp.zeros((ep_count, capacity, model_width), jnp.bfloat16)]
    all_to_all x2 -> x0, blocking collectives: 67.5 us -> none  [the longest x1 59.3 us: per_device(): lax.all_to_all(outbox, 'ep', split_axis=0, concat_axis=0, tiled=True)]
    pallas_call x0 -> x7, Pallas kernels: none -> 58 us  [the longest x1 14.2 us: hidden_of(): pl.pallas_call(partial(hidden_body, capacity=capacity, chunk=64), grid_sp...]
    dot_general x6 -> x2, matrix products: 38.9 us -> 3.33 us  [dot(): return jnp.dot(a, b, preferred_element_type=F32)]
    all_to_all x3 -> x0, local copies, waits for them, and re-layouts: 22.8 us -> none  [the longest x1 13.8 us: from_everyone(): lax.all_to_all(jnp.broadcast_to(x[None], (devices, *x.shape)), axis, 0, 0...]
  transfers between devices with their start and end apart: 5 -> 16, of which waited for: 4 -> 7; matrix products, arithmetic and copies ran while one was open for 10% -> 9% of each run, Pallas kernels for 0% -> 22%
where the time goes in v1:
time: 260 us; the launch traced here: 259 us
  waiting for transfers between devices  121 us (47%)
  Pallas kernels  58 us (22%)
  starting transfers between devices  34.1 us (13%)
  other arithmetic  17.6 us (7%)
  between operations  14.4 us (6%)
  local copies, waits for them, and re-layouts  10.7 us (4%)
  matrix products  3.33 us (1%)
    ppermute x11, waiting for transfers between devices, swapped(): lax.ppermute(x, axis, [(i, i ^ bits) for i in range(lax.axis_size(axis))])  105 us
    ppermute x11, starting transfers between devices, swapped(): lax.ppermute(x, axis, [(i, i ^ bits) for i in range(lax.axis_size(axis))])  15.4 us
    all_to_all x1, waiting for transfers between devices, per_device(): lax.all_to_all(expert_rows.reshape(ep_count, 2 * capacity, width // 2), '...  15.3 us
    pallas_call x1, Pallas kernels, hidden_of(): pl.pallas_call(partial(hidden_body, capacity=capacity, chunk=64), grid_sp...  14.2 us
    pallas_call x1, Pallas kernels, outbox_of(): pl.pallas_call(partial(outbox_body, capacity=capacity, chunk=16), grid_sp...  11.1 us
    pallas_call x1, Pallas kernels, down_of(): pl.pallas_call(partial(down_body, capacity=capacity), grid_spec=pltpu.Pre...  10.5 us
    all_to_all x1, starting transfers between devices, per_device(): lax.all_to_all(outbox.reshape(ep_count, 2 * capacity, width), 'ep', split...  9.6 us
    unnamed x48, local copies, waits for them, and re-layouts  8.11 us
  transfers between devices with their start and end apart: 16, of which 7 were waited for; matrix products, arithmetic and copies ran while one was open for 9% of the time, Pallas kernels for 22%

profile of v1, /device:TPU:0, one launch (start us, length us, event | category | flops | bytes accessed | tf_op | source)
XLA Modules:
  0.0 258.8 jit_solution(14871365594576781410)
XLA Ops:
  7.3 0.7 all-gather.3.cloned.1.call-update
  8.1 3.2 %collective-permute-start.1 = (s32[128,2]{1,0:T(8,128)S(1)}, s32[128,2]{1,0:T(8,128)S(1)}, u32[]{:S(2)}, u32[]{:S(2)}) collective-permute-start(s32[128,2]{1,0:T(8,128)S(1)} %copy.20.own.routes), channel_id=1, source_target_pairs={{0,2},{1,3},{2,0},{3,1},{4,6},{5,7},{6,4},{7,5},{8,10},{9,11},{10,... | collective-permute-start | bytes 3080 | tf_op jit(solution)/shard_map/ppermute | solution.py:22
  11.4 1.5 collective-permute-start
  12.9 0.6 pad_add_fusion.flags
  13.5 0.4 collective-permute-done.1.other
  14.0 0.6 copy-done.12
  14.6 11.1 %outbox.1 = bf16[768,4096]{1,0:T(8,128)(2,1)} custom-call(s32[2]{0:T(128)} %pad_add_fusion.flags, bf16[2,2,128,4096]{3,2,1,0:T(8,128)(2,1)} %bitcast.51, f32[1,4096]{1,0:T(1,128)} %bitcast.63, s32[128,2]{1,0:T(8,128)} %copy-done.10, s32[128,2]{1,0:T(8,128)} %copy-done.12), custom_call_target="tpu_custom_call" | custom-call | flops 1610612736 | bytes 8388608 | tf_op jit(solution)/shard_map/outbox/pallas_call | solution.py:95
  25.7 9.6 %all-to-all-start = ((bf16[32,24,4096]{2,1,0:T(8,128)(2,1)}), bf16[32,24,4096]{2,1,0:T(8,128)(2,1)}, u32[]{:S(2)}, u32[]{:S(2)}) async-start(bf16[32,24,4096]{2,1,0:T(8,128)(2,1)} %bitcast.50), calls=%async_computation.1 | async-start | bytes 12582912 | tf_op jit(solution)/shard_map/all_to_all | solution.py:395
  35.4 3.3 %fusion = f32[512]{0:T(512)S(1)} fusion(bf16[512,4096]{1,0:T(8,128)(2,1)} %param.24), kind=kLoop, calls=%fused_computation.2 | loop fusion | flops 6290944 | bytes 4196352 | tf_op jit(solution)/shard_map/reduce_sum | solution.py:407
  38.9 1.3 fusion.4
  40.2 0.3 copy-done.20
  40.5 2.0 fusion.6.hidden
  42.5 0.3 multiply_convert_fusion.1
  43.2 4.9 %fusion.42 = (f32[512]{0:T(512)S(1)}, f32[512]{0:T(512)S(1)}, f32[512,512]{1,0:T(8,128)S(1)}) fusion(f32[542,512]{1,0:T(8,128)S(1)} %maximum_convert_fusion, f32[512]{0:T(512)S(1)} %bitcast.74, f32[512]{0:T(512)S(1)} %bitcast.75, f32[512]{0:T(512)S(1)} %bitcast.77, f32[512]{0:T(512)S(1)} %bitcast.78, f32[512]{0:T(512)S(1)} %bitcast.79, f32[512]{0:T(512)S(1)} %bitcast.80, ...), kind=kLoop, calls=%fused_computation.93 | loop fusion | flops 17038336 | bytes 33624064 | tf_op jit(solution)/shard_map/reduce_sum | solution.py:401
  48.1 0.7 collective-permute-start.2
  48.9 2.7 %collective-permute-start.3 = (f32[2,512]{1,0:T(2,128)S(1)}, f32[2,512]{1,0:T(2,128)S(1)}, u32[]{:S(2)}, u32[]{:S(2)}) collective-permute-start(f32[2,512]{1,0:T(2,128)S(1)} %pad_maximum_fusion.3), channel_id=1, source_target_pairs={{0,2},{1,3},{2,0},{3,1},{4,6},{5,7},{6,4},{7,5},{8,10},{9,11},{10,... | collective-permute-start | bytes 12296 | tf_op jit(solution)/shard_map/ppermute | solution.py:22
  51.5 1.4 collective-permute-start.4
  52.9 5.2 %shared_product.1 = (bf16[256,2048]{1,0:T(8,128)(2,1)}, bf16[256,2048]{1,0:T(8,128)(2,1)}, bf16[256,2048]{1,0:T(8,128)(2,1)}, bf16[256,2048]{1,0:T(8,128)(2,1)}) custom-call(s32[2]{0:T(128)} %pad_add_fusion.flags, bf16[512,256]{1,0:T(8,128)(2,1)} %fusion.6.hidden, bf16[256,4096]{1,0:T(8,128)(2,1)} %down.2), custom_call_target="tpu_custom_call" | custom-call | flops 1073741824 | bytes 6291456 | tf_op jit(solution)/shard_map/shared_product/pallas_call | solution.py:266
  58.2 1.2 multiply_convert_fusion.a
  59.5 6.9 %shard_map.176 = bf16[512,4096]{1,0:T(8,128)(2,1)} custom-call(bf16[512,512]{1,0:T(8,128)(2,1)} %multiply_convert_fusion.a, bf16[512,4096]{1,0:T(8,128)(2,1)} %b.1), custom_call_target="tpu_custom_call" | custom-call | flops 2147483648 | bytes 8388608 | tf_op jit(solution)/shard_map/pallas_call | solution.py:236
  66.3 2.4 fusion.44
  69.4 2.0 collective-permute-start.6
  71.3 74.6 %collective-permute-done.5.first = bf16[4096,256]{1,0:T(8,128)(2,1)S(1)} collective-permute-done((bf16[4096,256]{1,0:T(8,128)(2,1)S(1)}, bf16[4096,256]{1,0:T(8,128)(2,1)S(1)}, u32[]{:S(2)}, u32[]{:S(2)}) %collective-permute-start.5) | collective-permute-done | bytes 2097184 | tf_op jit(solution)/shard_map/ppermute | solution.py:22
  145.9 1.4 copy-done.21
  147.3 1.4 copy-done.22
  148.7 14.2 %hidden.1 = (bf16[384,512]{1,0:T(8,128)(2,1)}, bf16[384,512]{1,0:T(8,128)(2,1)}) custom-call(s32[2]{0:T(128)} %pad_add_fusion.flags, bf16[768,4096]{1,0:T(8,128)(2,1)} %bitcast.40.arrived, bf16[4096,256]{1,0:T(8,128)(2,1)} %bitcast.54, bf16[4096,256]{1,0:T(8,128)(2,1)} %bitcast.56, bf16[4096,256]{1,0:T(8,128)(2,1)} %copy-done.21, bf16[4096,256]{1,0:T(8,128)(2,1)} %copy-done.22), custom_call_target="tpu_custom_call" | custom-call | flops 6442450944 | bytes 14680064 | tf_op jit(solution)/shard_map/hidden/pallas_call | solution.py:162
  162.9 2.1 collective-permute-start.7
  165.2 1.2 collective-permute-start.8
  166.4 17.0 %collective-permute-done.7.got = bf16[384,512]{1,0:T(8,128)(2,1)S(1)} collective-permute-done((bf16[384,512]{1,0:T(8,128)(2,1)}, bf16[384,512]{1,0:T(8,128)(2,1)S(1)}, u32[]{:S(2)}, u32[]{:S(2)}) %collective-permute-start.7) | collective-permute-done | bytes 393248 | tf_op jit(solution)/shard_map/ppermute | solution.py:22
  183.3 0.8 copy-done.11
  184.1 10.5 %down.3 = bf16[768,2048]{1,0:T(8,128)(2,1)} custom-call(s32[2]{0:T(128)} %pad_add_fusion.flags, bf16[384,512]{1,0:T(8,128)(2,1)} %get-tuple-element.24.kept, bf16[384,512]{1,0:T(8,128)(2,1)} %copy-done.11, bf16[1024,4096]{1,0:T(8,128)(2,1)} %bitcast.48, bf16[1024,4096]{1,0:T(8,128)(2,1)} %bitcast.49), custom_call_target="tpu_custom_call" | custom-call | flops 3221225472 | bytes 11534336 | tf_op jit(solution)/shard_map/down/pallas_call | solution.py:209
  194.6 7.6 %all-to-all-start.1 = ((bf16[32,24,2048]{2,1,0:T(8,128)(2,1)}), bf16[32,24,2048]{2,1,0:T(8,128)(2,1)}, u32[]{:S(2)}, u32[]{:S(2)}) async-start(bf16[32,24,2048]{2,1,0:T(8,128)(2,1)} %bitcast.52), calls=%async_computation.2 | async-start | bytes 6291456 | tf_op jit(solution)/shard_map/all_to_all | solution.py:434
  202.2 2.6 %collective-permute-done.10 = bf16[256,2048]{1,0:T(8,128)(2,1)S(1)} collective-permute-done((bf16[256,2048]{1,0:T(8,128)(2,1)}, bf16[256,2048]{1,0:T(8,128)(2,1)S(1)}, u32[]{:S(2)}, u32[]{:S(2)}) %collective-permute-start.10) | collective-permute-done | bytes 1048608 | tf_op jit(solution)/shard_map/ppermute | solution.py:22
  204.8 1.0 copy-done.7
  205.8 1.7 convert_add_fusion
  207.5 1.6 collective-permute-start.11
  209.1 1.6 convert_add_fusion.1
  210.7 1.3 copy-done.3
  212.1 0.3 collective-permute-start.9
  212.4 0.7 copy.22.weights
  213.2 2.4 portions.1
  215.5 5.8 %collective-permute-done.11 = bf16[128,2048]{1,0:T(8,128)(2,1)} collective-permute-done((bf16[128,2048]{1,0:T(8,128)(2,1)S(1)}, bf16[128,2048]{1,0:T(8,128)(2,1)}, u32[]{:S(2)}, u32[]{:S(2)}) %collective-permute-start.11) | collective-permute-done | bytes 524320 | tf_op jit(solution)/shard_map/ppermute | solution.py:22
  221.3 1.1 fusion.9
  222.4 4.2 %collective-permute-done.9 = bf16[128,2048]{1,0:T(8,128)(2,1)} collective-permute-done((bf16[128,2048]{1,0:T(8,128)(2,1)S(1)}, bf16[128,2048]{1,0:T(8,128)(2,1)}, u32[]{:S(2)}, u32[]{:S(2)}) %collective-permute-start.9) | collective-permute-done | bytes 524320 | tf_op jit(solution)/shard_map/ppermute | solution.py:22
  226.7 1.1 fusion.10
  227.8 1.1 pad_maximum_fusion.2.shared
  228.9 15.3 %all-to-all-done.1 = bf16[32,24,2048]{2,1,0:T(8,128)(2,1)} async-done(((bf16[32,24,2048]{2,1,0:T(8,128)(2,1)}), bf16[32,24,2048]{2,1,0:T(8,128)(2,1)}, u32[]{:S(2)}, u32[]{:S(2)}) %all-to-all-start.1) | async-done | bytes 3145760 | tf_op jit(solution)/shard_map/all_to_all | solution.py:434
  244.2 7.8 %mix.1 = bf16[128,4096]{1,0:T(8,128)(2,1)} custom-call(bf16[2,256,768]{2,1,0:T(8,128)(2,1)} %portions.1, bf16[768,2048]{1,0:T(8,128)(2,1)} %bitcast.45.returned, bf16[128,4096]{1,0:T(8,128)(2,1)} %pad_maximum_fusion.2.shared), custom_call_target="tpu_custom_call" | custom-call | flops 1610612736 | bytes 5242880 | tf_op jit(solution)/shard_map/mix/pallas_call | solution.py:325
  (67 shorter events, 1.9 us)
Async XLA Ops:
  7.2 31.5 %copy-start = (bf16[4096,256]{1,0:T(8,128)(2,1)S(1)}, bf16[4096,256]{1,0:T(8,128)(2,1)}, u32[]{:S(2)}) copy-start(bf16[4096,256]{1,0:T(8,128)(2,1)} %param.31) | copy-start | bytes 6291460
  7.2 0.8 copy-start.18
  7.2 4.2 %copy-start.9 = (bf16[512,512]{1,0:T(8,128)(2,1)S(1)}, bf16[512,512]{1,0:T(8,128)(2,1)}, u32[]{:S(2)}) copy-start(bf16[512,512]{1,0:T(8,128)(2,1)} %param.17) | copy-start | bytes 1572868
  7.2 4.1 %copy-start.8 = (bf16[512,512]{1,0:T(8,128)(2,1)S(1)}, bf16[512,512]{1,0:T(8,128)(2,1)}, u32[]{:S(2)}) copy-start(bf16[512,512]{1,0:T(8,128)(2,1)} %param.18) | copy-start | bytes 1572868
  7.2 5.7 %copy-start.13 = (f32[31,512]{1,0:T(8,128)S(1)}, f32[31,512]{1,0:T(8,128)}, u32[]{:S(2)}) copy-start(f32[31,512]{1,0:T(8,128)} %param.19) | copy-start | bytes 190468
  7.2 176.1 %all-gather.3.cloned.1.call-start = ((), (), s32[]{:S(2)}) async-start(), calls=%async_computation.4 | async-start | bytes 10485760 | tf_op jit(solution)/shard_map/all_gather | solution.py:381
  8.1 5.9 %copy-start.10 = (s32[128,2]{1,0:T(8,128)}, s32[128,2]{1,0:T(8,128)S(1)}, u32[]{:S(2)}) copy-start(s32[128,2]{1,0:T(8,128)S(1)} %copy.20.own.routes) | copy-start | bytes 3076
  8.1 5.8 %collective-permute-start.1 = (s32[128,2]{1,0:T(8,128)S(1)}, s32[128,2]{1,0:T(8,128)S(1)}, u32[]{:S(2)}, u32[]{:S(2)}) collective-permute-start(s32[128,2]{1,0:T(8,128)S(1)} %copy.20.own.routes), channel_id=1, source_target_pairs={{0,2},{1,3},{2,0},{3,1},{4,6},{5,7},{6,4},{7,5},{8,10},{9,11},{10,... | collective-permute-start | bytes 3080 | tf_op jit(solution)/shard_map/ppermute | solution.py:22
  11.4 31.4 %collective-permute-start = (bf16[30,512]{1,0:T(8,128)(2,1)S(1)}, bf16[30,512]{1,0:T(8,128)(2,1)S(1)}, u32[]{:S(2)}, u32[]{:S(2)}) collective-permute-start(bf16[30,512]{1,0:T(8,128)(2,1)S(1)} %multiply_convert_fusion.2), channel_id=1, source_target_pairs={{0,4},{4,8},{8,12},{12,16},{16,20},{20,24},{24,28},{28,32},{32,36}... | collective-permute-start | bytes 92168 | tf_op jit(solution)/shard_map/ppermute | solution.py:18
  14.0 0.6 copy-start.12
  25.7 13.0 %copy-start.14 = (f32[4096]{0:T(1024)S(1)}, f32[4096]{0:T(1024)}, u32[]{:S(2)}) copy-start(f32[4096]{0:T(1024)} %param.25) | copy-start | bytes 49156
  25.7 121.6 %all-to-all-start = ((bf16[32,24,4096]{2,1,0:T(8,128)(2,1)}), bf16[32,24,4096]{2,1,0:T(8,128)(2,1)}, u32[]{:S(2)}, u32[]{:S(2)}) async-start(bf16[32,24,4096]{2,1,0:T(8,128)(2,1)} %bitcast.50), calls=%async_computation.1 | async-start | bytes 12582912 | tf_op jit(solution)/shard_map/all_to_all | solution.py:395
  35.3 216.7 %reduce-scatter.2.cloned.1.call-start = ((), (), s32[]{:S(2)}) async-start(), calls=%async_computation.3 | async-start | bytes 5242880 | tf_op jit(solution)/shard_map/reduce_scatter | solution.py:425
  35.4 3.5 %copy-start.2 = (bf16[512,4096]{1,0:T(8,128)(2,1)S(1)}, bf16[512,4096]{1,0:T(8,128)(2,1)}, u32[]{:S(2)}) copy-start(bf16[512,4096]{1,0:T(8,128)(2,1)} %param.24) | copy-start | bytes 12582916
  38.9 1.6 copy-start.20
  42.5 0.7 copy-start.15
  48.1 10.1 %copy-start.16 = (f32[512]{0:T(512)S(1)}, f32[512]{0:T(512)}, u32[]{:S(2)}) copy-start(f32[512]{0:T(512)} %param.22) | copy-start | bytes 6148
  48.1 10.1 %copy-start.17 = (f32[512]{0:T(512)S(1)}, f32[512]{0:T(512)}, u32[]{:S(2)}) copy-start(f32[512]{0:T(512)} %param.21) | copy-start | bytes 6148
  48.1 10.0 %collective-permute-start.2 = (f32[2,512]{1,0:T(2,128)S(1)}, f32[2,512]{1,0:T(2,128)S(1)}, u32[]{:S(2)}, u32[]{:S(2)}) collective-permute-start(f32[2,512]{1,0:T(2,128)S(1)} %pad_maximum_fusion.3), channel_id=1, source_target_pairs={{0,1},{1,0},{2,3},{3,2},{4,5},{5,4},{6,7},{7,6},{8,9},{9,8},{10,11... | collective-permute-start | bytes 12296 | tf_op jit(solution)/shard_map/ppermute | solution.py:22
  48.9 9.3 %collective-permute-start.3 = (f32[2,512]{1,0:T(2,128)S(1)}, f32[2,512]{1,0:T(2,128)S(1)}, u32[]{:S(2)}, u32[]{:S(2)}) collective-permute-start(f32[2,512]{1,0:T(2,128)S(1)} %pad_maximum_fusion.3), channel_id=1, source_target_pairs={{0,2},{1,3},{2,0},{3,1},{4,6},{5,7},{6,4},{7,5},{8,10},{9,11},{10,... | collective-permute-start | bytes 12296 | tf_op jit(solution)/shard_map/ppermute | solution.py:22
  51.5 6.6 %collective-permute-start.4 = (f32[2,512]{1,0:T(2,128)S(1)}, f32[2,512]{1,0:T(2,128)S(1)}, u32[]{:S(2)}, u32[]{:S(2)}) collective-permute-start(f32[2,512]{1,0:T(2,128)S(1)} %pad_maximum_fusion.3), channel_id=1, source_target_pairs={{0,3},{1,2},{2,1},{3,0},{4,7},{5,6},{6,5},{7,4},{8,11},{9,10},{10,... | collective-permute-start | bytes 12296 | tf_op jit(solution)/shard_map/ppermute | solution.py:22
  69.0 76.9 %collective-permute-start.5 = (bf16[4096,256]{1,0:T(8,128)(2,1)S(1)}, bf16[4096,256]{1,0:T(8,128)(2,1)S(1)}, u32[]{:S(2)}, u32[]{:S(2)}) collective-permute-start(bf16[4096,256]{1,0:T(8,128)(2,1)S(1)} %pad_maximum_fusion), channel_id=1, source_target_pairs={{0,1},{1,0},{2,3},{3,2},{4,5},{5,4},{6,7},{7,6},{8,9},{9,8},{10,11... | collective-permute-start | bytes 6291464 | tf_op jit(solution)/shard_map/ppermute | solution.py:22
  69.4 78.0 %collective-permute-start.6 = (bf16[4096,256]{1,0:T(8,128)(2,1)S(1)}, bf16[4096,256]{1,0:T(8,128)(2,1)S(1)}, u32[]{:S(2)}, u32[]{:S(2)}) collective-permute-start(bf16[4096,256]{1,0:T(8,128)(2,1)S(1)} %pad_maximum_fusion.1), channel_id=1, source_target_pairs={{0,3},{1,2},{2,1},{3,0},{4,7},{5,6},{6,5},{7,4},{8,11},{9,10},{10,... | collective-permute-start | bytes 6291464 | tf_op jit(solution)/shard_map/ppermute | solution.py:22
  145.9 1.4 copy-start.21
  147.3 1.4 copy-start.22
  162.9 20.5 %collective-permute-start.7 = (bf16[384,512]{1,0:T(8,128)(2,1)}, bf16[384,512]{1,0:T(8,128)(2,1)S(1)}, u32[]{:S(2)}, u32[]{:S(2)}) collective-permute-start(bf16[384,512]{1,0:T(8,128)(2,1)} %get-tuple-element.25), channel_id=1, source_target_pairs={{0,2},{1,3},{2,0},{3,1},{4,6},{5,7},{6,4},{7,5},{8,10},{9,11},{10,... | collective-permute-start | bytes 1179656 | tf_op jit(solution)/shard_map/ppermute | solution.py:22
  165.0 39.8 %collective-permute-start.10 = (bf16[256,2048]{1,0:T(8,128)(2,1)}, bf16[256,2048]{1,0:T(8,128)(2,1)S(1)}, u32[]{:S(2)}, u32[]{:S(2)}) collective-permute-start(bf16[256,2048]{1,0:T(8,128)(2,1)} %get-tuple-element.29), channel_id=1, source_target_pairs={{0,3},{1,2},{2,1},{3,0},{4,7},{5,6},{6,5},{7,4},{8,11},{9,10},{10,... | collective-permute-start | bytes 3145736 | tf_op jit(solution)/shard_map/ppermute | solution.py:22
  165.2 43.9 %collective-permute-start.8 = (bf16[256,2048]{1,0:T(8,128)(2,1)}, bf16[256,2048]{1,0:T(8,128)(2,1)}, u32[]{:S(2)}, u32[]{:S(2)}) collective-permute-start(bf16[256,2048]{1,0:T(8,128)(2,1)} %get-tuple-element.27), channel_id=1, source_target_pairs={{0,1},{1,0},{2,3},{3,2},{4,5},{5,4},{6,7},{7,6},{8,9},{9,8},{10,11... | collective-permute-start | bytes 3145736 | tf_op jit(solution)/shard_map/ppermute | solution.py:22
  183.3 0.8 copy-start.11
  194.6 11.2 %copy-start.6 = (bf16[256,2048]{1,0:T(8,128)(2,1)S(1)}, bf16[256,2048]{1,0:T(8,128)(2,1)}, u32[]{:S(2)}) copy-start(bf16[256,2048]{1,0:T(8,128)(2,1)} %get-tuple-element.28) | copy-start | bytes 3145732
  194.6 49.6 %all-to-all-start.1 = ((bf16[32,24,2048]{2,1,0:T(8,128)(2,1)}), bf16[32,24,2048]{2,1,0:T(8,128)(2,1)}, u32[]{:S(2)}, u32[]{:S(2)}) async-start(bf16[32,24,2048]{2,1,0:T(8,128)(2,1)} %bitcast.52), calls=%async_computation.2 | async-start | bytes 6291456 | tf_op jit(solution)/shard_map/all_to_all | solution.py:434
  204.8 1.0 copy-start.7
  205.8 3.3 %copy-start.5 = (bf16[256,2048]{1,0:T(8,128)(2,1)S(1)}, bf16[256,2048]{1,0:T(8,128)(2,1)}, u32[]{:S(2)}) copy-start(bf16[256,2048]{1,0:T(8,128)(2,1)} %get-tuple-element.26) | copy-start | bytes 3145732
  207.5 13.8 %collective-permute-start.11 = (bf16[128,2048]{1,0:T(8,128)(2,1)S(1)}, bf16[128,2048]{1,0:T(8,128)(2,1)}, u32[]{:S(2)}, u32[]{:S(2)}) collective-permute-start(bf16[128,2048]{1,0:T(8,128)(2,1)S(1)} %slice.504), channel_id=1, source_target_pairs={{0,1},{1,0},{2,3},{3,2},{4,5},{5,4},{6,7},{7,6},{8,9},{9,8},{10,11... | collective-permute-start | bytes 1572872 | tf_op jit(solution)/shard_map/ppermute | solution.py:22
  209.1 3.3 %copy-start.19 = (f32[128,2]{0,1:T(2,128)S(1)}, f32[128,2]{0,1:T(2,128)}, u32[]{:S(2)}) copy-start(f32[128,2]{0,1:T(2,128)} %param.27) | copy-start | bytes 3076
  210.7 1.3 copy-start.3
  212.1 14.6 %collective-permute-start.9 = (bf16[128,2048]{1,0:T(8,128)(2,1)S(1)}, bf16[128,2048]{1,0:T(8,128)(2,1)}, u32[]{:S(2)}, u32[]{:S(2)}) collective-permute-start(bf16[128,2048]{1,0:T(8,128)(2,1)S(1)} %slice.505), channel_id=1, source_target_pairs={{0,3},{1,2},{2,1},{3,0},{4,7},{5,6},{6,5},{7,4},{8,11},{9,10},{10,... | collective-permute-start | bytes 1572872 | tf_op jit(solution)/shard_map/ppermute | solution.py:22
  215.5 11.2 %copy-start.4 = (f32[256,2048]{1,0:T(8,128)S(1)}, f32[256,2048]{1,0:T(8,128)}, u32[]{:S(2)}) copy-start(f32[256,2048]{1,0:T(8,128)} %copy-done.3) | copy-start | bytes 6291460
  244.2 7.8 %copy-start.1 = (bf16[4096,256]{1,0:T(8,128)(2,1)S(1)}, bf16[4096,256]{1,0:T(8,128)(2,1)}, u32[]{:S(2)}) copy-start(bf16[4096,256]{1,0:T(8,128)(2,1)} %param.31) | copy-start | bytes 6291460
Sparse Core Ops, SparseCore 0:
  9.7 109.9 all-gather.2
  122.6 67.4 reduce-scatter.1

commit v2 on v1

--- a/solution.py
+++ b/solution.py
@@ -93,7 +93,7 @@
     slots = experts * 2 * capacity
     here = 512
     return pl.pallas_call(
-        partial(outbox_body, capacity=capacity, chunk=16),
+        partial(outbox_body, capacity=capacity, chunk=32),
         grid_spec=pltpu.PrefetchScalarGridSpec(
             num_scalar_prefetch=1,
             grid=(width // here,),
@@ -174,76 +174,55 @@
     )(flags, arrived, gate, up, first, second)
 
 
-def down_body(flags, kept, got, left, right, out, whole, wide, *, capacity):
+def down_body(kept, got, *refs, capacity):
+    weights, (out, whole, wide) = refs[:10], refs[10:]
     units = whole.shape[1] // 4
     half = units // 2
 
     @pl.when(pl.program_id(0) == 0)
     def _():
-        k, g = kept[...], got[...]
-        by_distance = [
-            k[:, :units],
-            jnp.concatenate([k[:, units : units + half], g[:, units + half :]], axis=1),
-            g[:, :units],
-            jnp.concatenate([g[:, units : units + half], k[:, units + half :]], axis=1),
-        ]
-        odd, high = flags[0] == 1, flags[1] == 1
-        turned = [jnp.where(odd, by_distance[i ^ 1], by_distance[i]) for i in range(4)]
-        for i in range(4):
-            whole[:, i * units : (i + 1) * units] = jnp.where(high, turned[i ^ 2], turned[i])
-
-    for side, weight in enumerate((left, right)):
-        rows = dot(whole[...], weight[...])
+        whole[:, :units] = kept[:, :units]
+        whole[:, units : units + half] = kept[:, units : units + half]
+        whole[:, units + half : 2 * units] = got[:, units + half :]
+        whole[:, 2 * units : 3 * units] = got[:, :units]
+        whole[:, 3 * units : 3 * units + half] = got[:, units : units + half]
+        whole[:, 3 * units + half :] = kept[:, units + half :]
+
+    for side in range(2):
+        own, from_1, first_of_2, second_of_2, from_3 = (w[...] for w in weights[side::2])
+        from_2 = jnp.concatenate([first_of_2, second_of_2], axis=0)
+        rows = dot(whole[:, :units], own) + dot(whole[:, units : 2 * units], from_1)
+        rows += dot(whole[:, 2 * units : 3 * units], from_2) + dot(whole[:, 3 * units :], from_3)
         for expert in range(rows.shape[0] // capacity):
             at = (2 * expert + side) * capacity
             wide[at : at + capacity, :] = rows[expert * capacity : (expert + 1) * capacity, :]
     out[...] = wide[...].astype(BF16)
 
 
-def down_of(flags, kept, got, down, capacity):
-    rows, units = kept.shape[0], down.shape[0]
-    width = down.shape[1] // 2
+def down_of(kept, got, shards, capacity):
+    rows, units = kept.shape[0], sum(w.shape[0] for w in shards)
+    width = shards[0].shape[1] // 2
     step = 256
     count = width // step
-    whole = pl.BlockSpec(kept.shape, lambda n, f: (0, 0))
+    whole = pl.BlockSpec(kept.shape, lambda n: (0, 0))
+    specs, operands = [], []
+    for shard in shards:
+        for side in range(2):
+            specs.append(pl.BlockSpec((shard.shape[0], step), lambda n, side=side: (0, n + side * count)))
+            operands.append(shard)
     return pl.pallas_call(
         partial(down_body, capacity=capacity),
-        grid_spec=pltpu.PrefetchScalarGridSpec(
-            num_scalar_prefetch=1,
-            grid=(count,),
-            in_specs=[
-                whole,
-                whole,
-                pl.BlockSpec((units, step), lambda n, f: (0, n)),
-                pl.BlockSpec((units, step), lambda n, f: (0, n + count)),
-            ],
-            out_specs=pl.BlockSpec((2 * rows, step), lambda n, f: (0, n)),
-            scratch_shapes=[pltpu.VMEM((rows, units), BF16), pltpu.VMEM((2 * rows, step), F32)],
-        ),
+        grid=(count,),
+        in_specs=[whole, whole] + specs,
+        out_specs=pl.BlockSpec((2 * rows, step), lambda n: (0, n)),
+        scratch_shapes=[pltpu.VMEM((rows, units), BF16), pltpu.VMEM((2 * rows, step), F32)],
         out_shape=jax.ShapeDtypeStruct((2 * rows, width), BF16),
         cost_estimate=pl.CostEstimate(flops=4 * rows * units * width, bytes_accessed=4 * width * (rows + units), transcendentals=0),
         name="down",
-    )(flags, kept, got, down, down)
-
-
-def product_body(a, b, out):
-    out[...] = dot(a[...], b[...]).astype(BF16)
-
-
-def product_of(a, b):
-    rows, width = a.shape[0], b.shape[1]
-    block = 128
-    return pl.pallas_call(
-        product_body,
-        grid=(rows // block,),
-        in_specs=[pl.BlockSpec((block, a.shape[1]), lambda i: (i, 0)), pl.BlockSpec(b.shape, lambda i: (0, 0))],
-        out_specs=pl.BlockSpec((block, width), lambda i: (i, 0)),
-        out_shape=jax.ShapeDtypeStruct((rows, width), BF16),
-        cost_estimate=pl.CostEstimate(flops=2 * rows * width * b.shape[0], bytes_accessed=2 * width * (rows + b.shape[0]), transcendentals=0),
-    )(a, b)
-
-
-def shared_body(flags, hidden, down, send_1, keep_1, send_3, keep_3):
+    )(kept, got, *operands)
+
+
+def halves_body(flags, hidden, down, send_1, keep_1, send_3, keep_3):
     me = flags[0] + 2 * flags[1]
     block, width = send_1.shape[0] // 2, send_1.shape[1]
     targets = (
@@ -259,12 +238,12 @@
             out[place * block : (place + 1) * block, :] = product.astype(BF16)
 
 
-def shared_parts_of(flags, hidden, down):
+def halves_of(flags, hidden, down):
     rows, width = hidden.shape[0], down.shape[1]
     out = jax.ShapeDtypeStruct((rows // 2, width // 2), BF16)
     whole = pl.BlockSpec(out.shape, lambda i, f: (0, 0))
     return pl.pallas_call(
-        shared_body,
+        halves_body,
         grid_spec=pltpu.PrefetchScalarGridSpec(
             num_scalar_prefetch=1,
             grid=(1,),
@@ -273,7 +252,6 @@
         ),
         out_shape=[out] * 4,
         cost_estimate=pl.CostEstimate(flops=2 * rows * width * down.shape[0], bytes_accessed=2 * width * (rows + down.shape[0]), transcendentals=0),
-        name="shared_product",
     )(flags, hidden, down)
 
 
@@ -311,30 +289,60 @@
     )(routes, weights)
 
 
-def mix_body(portions, returned, shared, out):
-    block = out.shape[0]
-    both = dot(portions[pl.program_id(1)], returned[...])
-    out[...] = (shared[...].astype(F32) + (both[:block] + both[block:])).astype(BF16)
+def mix_body(portions, returned, *refs):
+    shared, out = refs[:-1], refs[-1]
+    block, step = out.shape[0], returned.shape[1]
+    at = pl.program_id(0) * step
+    both = dot(portions[...], returned[...])
+    for side in range(2):
+        total = both[2 * side * block : (2 * side + 1) * block] + both[(2 * side + 1) * block : (2 * side + 2) * block]
+        for part in shared[3 * side : 3 * side + 3]:
+            total += part[...].astype(F32)
+        here = pl.multiple_of(at + side * (out.shape[1] // 2), step)
+        out[:, pl.ds(here, step)] = total.astype(BF16)
 
 
 def mixed_of(portions, returned, shared):
     slots, width = returned.shape
-    block = shared.shape[0]
+    block = portions.shape[1] // 2
     step = 512
     count = width // step
+    portions = portions.reshape(4 * block, slots)
     return pl.pallas_call(
         mix_body,
-        grid=(count, 2),
+        grid=(count,),
         in_specs=[
-            pl.BlockSpec(portions.shape, lambda n, h: (0, 0, 0)),
-            pl.BlockSpec((slots, step), lambda n, h: (0, n)),
-            pl.BlockSpec((block, step), lambda n, h: (0, h * count + n)),
-        ],
-        out_specs=pl.BlockSpec((block, step), lambda n, h: (0, h * count + n)),
+            pl.BlockSpec(portions.shape, lambda n: (0, 0)),
+            pl.BlockSpec((slots, step), lambda n: (0, n)),
+        ]
+        + [pl.BlockSpec((block, step), lambda n: (0, n))] * 6,
+        out_specs=pl.BlockSpec((block, 2 * width), lambda n: (0, 0)),
         out_shape=jax.ShapeDtypeStruct((block, 2 * width), BF16),
-        cost_estimate=pl.CostEstimate(flops=8 * block * slots * width, bytes_accessed=2 * width * (slots + 4 * block), transcendentals=0),
+        cost_estimate=pl.CostEstimate(flops=8 * block * slots * width, bytes_accessed=2 * width * (slots + 8 * block), transcendentals=0),
         name="mix",
-    )(portions, returned, shared)
+    )(portions, returned, *shared)
+
+
+def sum_body(*refs):
+    parts, out = refs[:-1], refs[-1]
+    width = out.shape[1] // 2
+    for side in range(2):
+        total = sum(part[...].astype(F32) for part in parts[3 * side : 3 * side + 3])
+        out[:, side * width : (side + 1) * width] = total.astype(BF16)
+
+
+def sum_of(parts):
+    block, width = parts[2].shape
+    rows = 32
+    return pl.pallas_call(
+        sum_body,
+        grid=(block // rows,),
+        in_specs=[pl.BlockSpec((rows, width), lambda i: (i, 0))] * 6,
+        out_specs=pl.BlockSpec((rows, 2 * width), lambda i: (i, 0)),
+        out_shape=jax.ShapeDtypeStruct((block, 2 * width), BF16),
+        cost_estimate=pl.CostEstimate(flops=4 * block * width, bytes_accessed=16 * block * width, transcendentals=0),
+        name="sum",
+    )(*parts)
 
 
 def gated_of(value_in, gate_in):
@@ -348,6 +356,17 @@
     for tap_index in range(conv_taps.shape[0]):
         filtered = filtered + conv_taps[tap_index][None, :] * padded[tap_index : tap_index + length]
     return filtered
+
+
+def two_swaps(send_1, keep_1, send_3, keep_3):
+    block = send_1.shape[0] // 2
+    left_1 = swapped(send_1, "tp", 1)
+    right_1 = swapped(send_3, "tp", 3)
+    left_on = (keep_1[block:].astype(F32) + left_1[block:].astype(F32)).astype(BF16)
+    right_on = (keep_3[block:].astype(F32) + right_1[block:].astype(F32)).astype(BF16)
+    left_2 = swapped(left_on, "tp", 3)
+    right_2 = swapped(right_on, "tp", 1)
+    return keep_1, left_1, left_2, keep_3, right_1, right_2
 
 
 def per_device(
@@ -378,7 +397,7 @@
     width = tokens_b.shape[1]
     gate_local, up_local, down_local = expert_gate[0], expert_up[0], expert_down[0]
     half = gate_local.shape[1] // 2
-    down_all = lax.all_gather(down_local, "tp", axis=0, tiled=True)
+    down_half = down_local.shape[0] // 2
 
     other_routes = swapped(routes, "tp", 2)
 
@@ -386,16 +405,23 @@
     tail = gated_of(value_in[rim:], gate_in[rim:])
     before = shifted(tail, "ep", 1)
 
-    first = jnp.concatenate([gate_local[:, :half], up_local[:, :half]], axis=1)
-    second = jnp.concatenate([gate_local[:, half:], up_local[:, half:]], axis=1)
-    first_of_1 = swapped(first, "tp", 1)
-    second_of_3 = swapped(second, "tp", 3)
+    down_1 = swapped(down_local, "tp", 1)
+    down_3 = swapped(down_local, "tp", 3)
 
     outbox = outbox_of(flags, tokens_b, norm_gain, routes, other_routes, ep_count, capacity)
     arrived = lax.all_to_all(
         outbox.reshape(ep_count, 2 * capacity, width), "ep", split_axis=0, concat_axis=0, tiled=True
     ).reshape(2 * capacity * ep_count, width)
-    tokens_b, value_in, gate_in, outbox = lax.optimization_barrier((tokens_b, value_in, gate_in, outbox))
+    tokens_b, value_in, gate_in, gate_sent, up_sent, outbox = lax.optimization_barrier(
+        (tokens_b, value_in, gate_in, gate_local, up_local, outbox)
+    )
+
+    first = jnp.concatenate([gate_sent[:, :half], up_sent[:, :half]], axis=1)
+    second = jnp.concatenate([gate_sent[:, half:], up_sent[:, half:]], axis=1)
+    first_of_1 = swapped(first, "tp", 1)
+    second_of_3 = swapped(second, "tp", 3)
+    down_2a = swapped(down_3[:down_half], "tp", 1)
+    down_2b = swapped(down_1[down_half:], "tp", 3)
 
     filtered = convolved(before, gated_of(value_in, gate_in), conv_taps, conv_bias)
     sums = jnp.stack([jnp.sum(filtered, axis=1), jnp.sum(filtered * filtered, axis=1)])
@@ -408,7 +434,7 @@
         * norm_gain
     ).astype(BF16)
     hidden_shared = gated_product(dot(normed_b, shared_gate), dot(normed_b, shared_up))
-    send_1, keep_1, send_3, keep_3 = shared_parts_of(flags, hidden_shared, shared_down)
+    send_1, keep_1, send_3, keep_3 = halves_of(flags, hidden_shared, shared_down)
 
     *other_sums, hidden_shared, send_1, send_3 = lax.optimization_barrier(
         (*other_sums, hidden_shared, send_1, send_3)
@@ -421,29 +447,22 @@
         variance[:, None] + EPSILON
     ) * ln_gain + ln_bias
     activated = jax.nn.silu(normed_a).astype(BF16)
-    mixer_parts = product_of(activated, out_proj)
-    mixer_rows = lax.psum_scatter(mixer_parts, "tp", scatter_dimension=0, tiled=True)
+    mixer_parts = halves_of(flags, activated, out_proj)
 
     kept, sent = hidden_of(flags, arrived, gate_local, up_local, first_of_1, second_of_3, capacity)
     got = swapped(sent, "tp", 2)
 
-    left_1 = swapped(send_1, "tp", 1)
-    right_1 = swapped(send_3, "tp", 3)
-
-    expert_rows = down_of(flags, kept, got, down_all, capacity)
+    shared_sums = two_swaps(send_1, keep_1, send_3, keep_3)
+    mixer_sums = two_swaps(*mixer_parts)
+
+    expert_rows = down_of(kept, got, (down_local, down_1, down_2a, down_2b, down_3), capacity)
     returned = lax.all_to_all(
         expert_rows.reshape(ep_count, 2 * capacity, width // 2), "ep", split_axis=0, concat_axis=0, tiled=True
     ).reshape(2 * capacity * ep_count, width // 2)
-    left_sum = keep_1.astype(F32) + left_1.astype(F32)
-    right_sum = keep_3.astype(F32) + right_1.astype(F32)
-    left_on, right_on = left_sum[rows_own:].astype(BF16), right_sum[rows_own:].astype(BF16)
-    left_2 = swapped(left_on, "tp", 3)
-    right_2 = swapped(right_on, "tp", 1)
-    shared_rows = jnp.concatenate(
-        [left_sum[:rows_own] + left_2.astype(F32), right_sum[:rows_own] + right_2.astype(F32)], axis=1
-    ).astype(BF16)
     portions = portions_of(routes, route_weights, ep_count, capacity)
-    experts_out = mixed_of(portions, returned, shared_rows)
+    experts_out = mixed_of(portions, returned, shared_sums)
+    *mixer_sums, experts_out = lax.optimization_barrier((*mixer_sums, experts_out))
+    mixer_rows = sum_of(mixer_sums)
     return (mixer_rows, experts_out)
 
 

time: 260 us -> 278 us (1.069)
  waiting for transfers between devices: 121 us -> 142 us
  between operations: 14.4 us -> 0.92 us
  starting transfers between devices: 34.1 us -> 41.2 us
    ppermute x11 -> x19, waiting for transfers between devices: 105 us -> 141 us  [swapped(): lax.ppermute(x, axis, [(i, i ^ bits) for i in range(lax.axis_size(axis))])]
    all_to_all x1, waiting for transfers between devices: 15.3 us -> 0.01 us  [per_device(): lax.all_to_all(expert_rows.reshape(ep_count, 2 * capacity, width // 2), '...]
    ppermute x11 -> x19, starting transfers between devices: 15.4 us -> 24.2 us  [swapped(): lax.ppermute(x, axis, [(i, i ^ bits) for i in range(lax.axis_size(axis))])]
    convert_element_type x0 -> x4, other arithmetic: none -> 6.09 us  [the longest x2 3.06 us: two_swaps(): (keep_3[block:].astype(F32) + right_1[block:].astype(F32)).astype(BF16)]
    unnamed x48 -> x50, local copies, waits for them, and re-layouts: 8.11 us -> 3.12 us
    slice x3, local copies, waits for them, and re-layouts: 2.57 us -> 6.07 us  [the longest x1 2.45 us: per_device(): second = jnp.concatenate([gate_sent[:, half:], up_sent[:, half:]], axis=1)]
    add x2 -> x0, other arithmetic: 3.23 us -> none  [the longest x1 1.65 us: per_device(): right_sum = keep_3.astype(F32) + right_1.astype(F32)]
    pallas_call x5 -> x6, Pallas kernels: 41.5 us -> 42 us  [the longest x2 11.7 us: halves_of(): pl.pallas_call(halves_body, grid_spec=pltpu.PrefetchScalarGridSpec(num_sc...]
  transfers between devices with their start and end apart: 16 -> 22, of which waited for: 7 -> 12; matrix products, arithmetic and copies ran while one was open for 9% -> 12% of each run, Pallas kernels for 22% -> 20%
where the time goes in v2:
time: 278 us; the launch traced here: 276 us
  waiting for transfers between devices  142 us (51%)
  Pallas kernels  58.4 us (21%)
  starting transfers between devices  41.2 us (15%)
  other arithmetic  19.1 us (7%)
  local copies, waits for them, and re-layouts  11.4 us (4%)
  matrix products  3.43 us (1%)
    ppermute x19, waiting for transfers between devices, swapped(): lax.ppermute(x, axis, [(i, i ^ bits) for i in range(lax.axis_size(axis))])  141 us
    ppermute x19, starting transfers between devices, swapped(): lax.ppermute(x, axis, [(i, i ^ bits) for i in range(lax.axis_size(axis))])  24.2 us
    pallas_call x1, Pallas kernels, hidden_of(): pl.pallas_call(partial(hidden_body, capacity=capacity, chunk=64), grid_sp...  14 us
    pallas_call x2, Pallas kernels, halves_of(): pl.pallas_call(halves_body, grid_spec=pltpu.PrefetchScalarGridSpec(num_sc...  11.7 us
    pallas_call x1, Pallas kernels, down_of(): pl.pallas_call(partial(down_body, capacity=capacity), grid=(count,), in_s...  10.2 us
    pallas_call x1, Pallas kernels, outbox_of(): pl.pallas_call(partial(outbox_body, capacity=capacity, chunk=32), grid_sp...  9.92 us
    all_to_all x1, starting transfers between devices, per_device(): lax.all_to_all(outbox.reshape(ep_count, 2 * capacity, width), 'ep', split...  8.55 us
    all_to_all x1, starting transfers between devices, per_device(): lax.all_to_all(expert_rows.reshape(ep_count, 2 * capacity, width // 2), '...  7.16 us
  transfers between devices with their start and end apart: 22, of which 12 were waited for; matrix products, arithmetic and copies ran while one was open for 12% of the time, Pallas kernels for 20%

profile of v2, /device:TPU:0, one launch (start us, length us, event | category | flops | bytes accessed | tf_op | source)
XLA Modules:
  0.0 276.3 jit_solution(4888126759297311768)
XLA Ops:
  0.6 2.9 %collective-permute-start.13 = (bf16[256,4096]{1,0:T(8,128)(2,1)}, bf16[256,4096]{1,0:T(8,128)(2,1)}, u32[]{:S(2)}, u32[]{:S(2)}) collective-permute-start(bf16[256,4096]{1,0:T(8,128)(2,1)} %bitcast.52), channel_id=1, source_target_pairs={{0,3},{1,2},{2,1},{3,0},{4,7},{5,6},{6,5},{7,4},{8,11},{9,10},{10,... | collective-permute-start | bytes 6291464 | tf_op jit(solution)/shard_map/ppermute | solution.py:22
  4.6 1.7 collective-permute-start.1
  7.1 1.3 collective-permute-start
  8.4 1.1 fusion.44
  10.2 41.9 %collective-permute-done.1.other = s32[128,2]{1,0:T(8,128)S(1)} collective-permute-done((s32[128,2]{1,0:T(8,128)S(1)}, s32[128,2]{1,0:T(8,128)S(1)}, u32[]{:S(2)}, u32[]{:S(2)}) %collective-permute-start.1) | collective-permute-done | bytes 1056 | tf_op jit(solution)/shard_map/ppermute | solution.py:22
  52.7 9.9 %outbox.1 = bf16[768,4096]{1,0:T(8,128)(2,1)} custom-call(s32[2]{0:T(128)} %pad_add_fusion.flags, bf16[2,2,128,4096]{3,2,1,0:T(8,128)(2,1)} %bitcast.50, f32[1,4096]{1,0:T(1,128)} %bitcast.67, s32[128,2]{1,0:T(8,128)} %copy-done.14, s32[128,2]{1,0:T(8,128)} %copy-done.17), custom_call_target="tpu_custom_call" | custom-call | flops 1610612736 | bytes 8388608 | tf_op jit(solution)/shard_map/outbox/pallas_call | solution.py:95
  62.7 8.6 %all-to-all-start = ((bf16[32,24,4096]{2,1,0:T(8,128)(2,1)}), bf16[32,24,4096]{2,1,0:T(8,128)(2,1)}, u32[]{:S(2)}, u32[]{:S(2)}) async-start(bf16[32,24,4096]{2,1,0:T(8,128)(2,1)} %bitcast.49), calls=%async_computation | async-start | bytes 12582912 | tf_op jit(solution)/shard_map/all_to_all | solution.py:412
  71.2 1.1 fusion.45
  72.3 2.4 fusion.42
  74.8 1.6 pad_maximum_fusion.1
  76.4 2.8 collective-permute-start.10
  79.2 1.6 pad_maximum_fusion
  81.1 0.9 fusion
  82.2 5.7 %fusion.40 = (f32[512]{0:T(512)S(1)}, f32[512]{0:T(512)S(1)}, f32[512,512]{1,0:T(8,128)}) fusion(f32[542,512]{1,0:T(8,128)S(1)} %maximum_convert_fusion, f32[512]{0:T(512)S(1)} %bitcast.97, f32[512]{0:T(512)S(1)} %bitcast.98, f32[512]{0:T(512)S(1)} %bitcast.69, f32[512]{0:T(512)S(1)} %bitcast.70, f32[512]{0:T(512)S(1)} %bitcast.71, f32[512]{0:T(512)S(1)} %bitcast.72, ...), kind=kLoop, calls=%fused_computation.88 | loop fusion | flops 17038336 | bytes 33624064 | tf_op jit(solution)/shard_map/reduce_sum | solution.py:427
  87.9 2.1 collective-permute-start.2
  90.0 1.4 fusion.4
  91.4 37.2 %collective-permute-done.2 = f32[2,512]{1,0:T(2,128)S(1)} collective-permute-done((f32[2,512]{1,0:T(2,128)S(1)}, f32[2,512]{1,0:T(2,128)S(1)}, u32[]{:S(2)}, u32[]{:S(2)}) %collective-permute-start.2) | collective-permute-done | bytes 4128 | tf_op jit(solution)/shard_map/ppermute | solution.py:22
  128.8 2.1 fusion.6.hidden
  130.9 2.8 %collective-permute-done.3 = f32[2,512]{1,0:T(2,128)S(1)} collective-permute-done((f32[2,512]{1,0:T(2,128)S(1)}, f32[2,512]{1,0:T(2,128)S(1)}, u32[]{:S(2)}, u32[]{:S(2)}) %collective-permute-start.3) | collective-permute-done | bytes 4128 | tf_op jit(solution)/shard_map/ppermute | solution.py:22
  134.2 5.2 %shard_map.176 = (bf16[256,2048]{1,0:T(8,128)(2,1)}, bf16[256,2048]{1,0:T(8,128)(2,1)}, bf16[256,2048]{1,0:T(8,128)(2,1)}, bf16[256,2048]{1,0:T(8,128)(2,1)}) custom-call(s32[2]{0:T(128)} %pad_add_fusion.flags, bf16[512,256]{1,0:T(8,128)(2,1)} %fusion.6.hidden, bf16[256,4096]{1,0:T(8,128)(2,1)} %down.3), custom_call_target="tpu_custom_call" | custom-call | flops 1073741824 | bytes 6291456 | tf_op jit(solution)/shard_map/pallas_call | solution.py:245
  139.4 2.8 %collective-permute-start.18 = (bf16[256,2048]{1,0:T(8,128)(2,1)}, bf16[256,2048]{1,0:T(8,128)(2,1)}, u32[]{:S(2)}, u32[]{:S(2)}) collective-permute-start(bf16[256,2048]{1,0:T(8,128)(2,1)} %get-tuple-element.48), channel_id=1, source_target_pairs={{0,3},{1,2},{2,1},{3,0},{4,7},{5,6},{6,5},{7,4},{8,11},{9,10},{10,... | collective-permute-start | bytes 3145736 | tf_op jit(solution)/shard_map/ppermute | solution.py:22
  142.2 1.3 slice.355
  143.5 1.4 collective-permute-start.14
  145.0 2.3 slice.356
  147.9 1.2 all-to-all-done
  149.1 14.0 %hidden.1 = (bf16[384,512]{1,0:T(8,128)(2,1)}, bf16[384,512]{1,0:T(8,128)(2,1)}) custom-call(s32[2]{0:T(128)} %pad_add_fusion.flags, bf16[768,4096]{1,0:T(8,128)(2,1)} %bitcast.43.arrived, bf16[4096,256]{1,0:T(8,128)(2,1)} %bitcast.58, bf16[4096,256]{1,0:T(8,128)(2,1)} %bitcast.60, bf16[4096,256]{1,0:T(8,128)(2,1)} %collective-permute-done.9.first, ...), custom_call_target="tpu_custom_call" | custom-call | flops 6442450944 | bytes 14680064 | tf_op jit(solution)/shard_map/hidden/pallas_call | solution.py:162
  163.1 1.9 collective-permute-start.11
  165.1 23.0 %collective-permute-done.14.refs_4_.refs_5_ = bf16[128,4096]{1,0:T(8,128)(2,1)S(1)} collective-permute-done((bf16[128,4096]{1,0:T(8,128)(2,1)S(1)}, bf16[128,4096]{1,0:T(8,128)(2,1)S(1)}, u32[]{:S(2)}, u32[]{:S(2)}) %collective-permute-start.14) | collective-permute-done | bytes 1048608 | tf_op jit(solution)/shard_map/ppermute | solution.py:22
  188.1 6.0 %collective-permute-done.15.refs_6_.refs_7_ = bf16[128,4096]{1,0:T(8,128)(2,1)S(1)} collective-permute-done((bf16[128,4096]{1,0:T(8,128)(2,1)}, bf16[128,4096]{1,0:T(8,128)(2,1)S(1)}, u32[]{:S(2)}, u32[]{:S(2)}) %collective-permute-start.15) | collective-permute-done | bytes 1048608 | tf_op jit(solution)/shard_map/ppermute | solution.py:22
  194.1 1.8 collective-permute-done.11.got
  195.9 10.2 %down.5 = bf16[768,2048]{1,0:T(8,128)(2,1)} custom-call(bf16[384,512]{1,0:T(8,128)(2,1)} %get-tuple-element.43.kept, bf16[384,512]{1,0:T(8,128)(2,1)} %collective-permute-done.11.got, bf16[256,4096]{1,0:T(8,128)(2,1)} %bitcast.54, bf16[256,4096]{1,0:T(8,128)(2,1)} %bitcast.55, bf16[256,4096]{1,0:T(8,128)(2,1)} %collective-permute-done.12.refs_2_.refs_3_, ...), custom_call_target="tpu_custom_call" | custom-call | flops 3221225472 | bytes 11534336 | tf_op jit(solution)/shard_map/down/pallas_call | solution.py:213
  206.1 7.2 %all-to-all-start.1 = ((bf16[32,24,2048]{2,1,0:T(8,128)(2,1)}), bf16[32,24,2048]{2,1,0:T(8,128)(2,1)}, u32[]{:S(2)}, u32[]{:S(2)}) async-start(bf16[32,24,2048]{2,1,0:T(8,128)(2,1)} %bitcast.51), calls=%async_computation.1 | async-start | bytes 6291456 | tf_op jit(solution)/shard_map/all_to_all | solution.py:459
  213.3 1.2 multiply_convert_fusion.hidden
  214.6 6.6 %shard_map.177 = (bf16[256,2048]{1,0:T(8,128)(2,1)}, bf16[256,2048]{1,0:T(8,128)(2,1)}, bf16[256,2048]{1,0:T(8,128)(2,1)}, bf16[256,2048]{1,0:T(8,128)(2,1)}) custom-call(s32[2]{0:T(128)} %pad_add_fusion.flags, bf16[512,512]{1,0:T(8,128)(2,1)} %multiply_convert_fusion.hidden, bf16[512,4096]{1,0:T(8,128)(2,1)} %down.4), custom_call_target="tpu_custom_call" | custom-call | flops 2147483648 | bytes 8388608 | tf_op jit(solution)/shard_map/pallas_call | solution.py:245
  221.1 2.8 %collective-permute-start.7 = (bf16[256,2048]{1,0:T(8,128)(2,1)}, bf16[256,2048]{1,0:T(8,128)(2,1)S(1)}, u32[]{:S(2)}, u32[]{:S(2)}) collective-permute-start(bf16[256,2048]{1,0:T(8,128)(2,1)} %get-tuple-element.40), channel_id=1, source_target_pairs={{0,3},{1,2},{2,1},{3,0},{4,7},{5,6},{6,5},{7,4},{8,11},{9,10},{10,... | collective-permute-start | bytes 3145736 | tf_op jit(solution)/shard_map/ppermute | solution.py:22
  223.9 2.0 add_convert_fusion.1
  226.6 2.0 add_convert_fusion
  228.6 1.3 collective-permute-start.19
  229.9 18.7 %collective-permute-done.7.refs_4_ = bf16[256,2048]{1,0:T(8,128)(2,1)S(1)} collective-permute-done((bf16[256,2048]{1,0:T(8,128)(2,1)}, bf16[256,2048]{1,0:T(8,128)(2,1)S(1)}, u32[]{:S(2)}, u32[]{:S(2)}) %collective-permute-start.7) | collective-permute-done | bytes 1048608 | tf_op jit(solution)/shard_map/ppermute | solution.py:22
  248.6 1.1 add_convert_fusion.2
  250.2 1.1 add_convert_fusion.3
  251.3 2.3 collective-permute-start.6
  254.3 2.3 portions.1
  256.7 3.2 %collective-permute-done.17.refs_2_ = bf16[128,2048]{1,0:T(8,128)(2,1)S(1)} collective-permute-done((bf16[128,2048]{1,0:T(8,128)(2,1)}, bf16[128,2048]{1,0:T(8,128)(2,1)S(1)}, u32[]{:S(2)}, u32[]{:S(2)}) %collective-permute-start.17) | collective-permute-done | bytes 524320 | tf_op jit(solution)/shard_map/ppermute | solution.py:22
  259.8 1.7 collective-permute-done.19.refs_5_
  261.5 6.3 %mix.1 = bf16[128,4096]{1,0:T(8,128)(2,1)} custom-call(bf16[512,768]{1,0:T(8,128)(2,1)} %bitcast.56, bf16[768,2048]{1,0:T(8,128)(2,1)} %bitcast.46.returned, bf16[256,2048]{1,0:T(8,128)(2,1)} %get-tuple-element.45.refs_0_, bf16[256,2048]{1,0:T(8,128)(2,1)} %collective-permute-done.16.refs_1_, bf16[128,2048]{1,0:T(8,128)(2,1)} %copy-done.15, ...), custom_call_target="tpu_custom_call" | custom-call | flops 1610612736 | bytes 7340032 | tf_op jit(solution)/shard_map/mix/pallas_call | solution.py:311
  267.8 3.8 %collective-permute-done.8.refs_5_ = bf16[128,2048]{1,0:T(8,128)(2,1)S(1)} collective-permute-done((bf16[128,2048]{1,0:T(8,128)(2,1)}, bf16[128,2048]{1,0:T(8,128)(2,1)S(1)}, u32[]{:S(2)}, u32[]{:S(2)}) %collective-permute-start.8) | collective-permute-done | bytes 524320 | tf_op jit(solution)/shard_map/ppermute | solution.py:22
  272.4 4.0 %sum.1 = bf16[128,4096]{1,0:T(8,128)(2,1)} custom-call(bf16[256,2048]{1,0:T(8,128)(2,1)} %get-tuple-element.49.refs_0_, bf16[256,2048]{1,0:T(8,128)(2,1)} %copy-done.11, bf16[128,2048]{1,0:T(8,128)(2,1)} %collective-permute-done.6.refs_2_, bf16[256,2048]{1,0:T(8,128)(2,1)} %get-tuple-element.52.refs_3_, bf16[256,2048]{1,0:T(8,128)(2,1)} %copy-done.10, ...), custom_call_target="tpu_custom_call" | custom-call | flops 1048576 | bytes 4194304 | tf_op jit(solution)/shard_map/sum/pallas_call | solution.py:337
  (79 shorter events, 7.8 us)
Async XLA Ops:
  0.6 89.4 %copy-start = (bf16[4096,256]{1,0:T(8,128)(2,1)S(1)}, bf16[4096,256]{1,0:T(8,128)(2,1)}, u32[]{:S(2)}) copy-start(bf16[4096,256]{1,0:T(8,128)(2,1)} %param.31) | copy-start | bytes 6291460
  0.6 138.7 %collective-permute-start.13 = (bf16[256,4096]{1,0:T(8,128)(2,1)}, bf16[256,4096]{1,0:T(8,128)(2,1)}, u32[]{:S(2)}, u32[]{:S(2)}) collective-permute-start(bf16[256,4096]{1,0:T(8,128)(2,1)} %bitcast.52), channel_id=1, source_target_pairs={{0,3},{1,2},{2,1},{3,0},{4,7},{5,6},{6,5},{7,4},{8,11},{9,10},{10,... | collective-permute-start | bytes 6291464 | tf_op jit(solution)/shard_map/ppermute | solution.py:22
  3.6 139.9 %collective-permute-start.12 = (bf16[256,4096]{1,0:T(8,128)(2,1)}, bf16[256,4096]{1,0:T(8,128)(2,1)}, u32[]{:S(2)}, u32[]{:S(2)}) collective-permute-start(bf16[256,4096]{1,0:T(8,128)(2,1)} %bitcast.53), channel_id=1, source_target_pairs={{0,1},{1,0},{2,3},{3,2},{4,5},{5,4},{6,7},{7,6},{8,9},{9,8},{10,11... | collective-permute-start | bytes 6291464 | tf_op jit(solution)/shard_map/ppermute | solution.py:22
  4.6 47.5 %copy-start.14 = (s32[128,2]{1,0:T(8,128)}, s32[128,2]{1,0:T(8,128)S(1)}, u32[]{:S(2)}) copy-start(s32[128,2]{1,0:T(8,128)S(1)} %copy.20.own.routes) | copy-start | bytes 3076
  4.6 47.5 %collective-permute-start.1 = (s32[128,2]{1,0:T(8,128)S(1)}, s32[128,2]{1,0:T(8,128)S(1)}, u32[]{:S(2)}, u32[]{:S(2)}) collective-permute-start(s32[128,2]{1,0:T(8,128)S(1)} %copy.20.own.routes), channel_id=1, source_target_pairs={{0,2},{1,3},{2,0},{3,1},{4,6},{5,7},{6,4},{7,5},{8,10},{9,11},{10,... | collective-permute-start | bytes 3080 | tf_op jit(solution)/shard_map/ppermute | solution.py:22
  7.1 74.9 %collective-permute-start = (bf16[30,512]{1,0:T(8,128)(2,1)S(1)}, bf16[30,512]{1,0:T(8,128)(2,1)S(1)}, u32[]{:S(2)}, u32[]{:S(2)}) collective-permute-start(bf16[30,512]{1,0:T(8,128)(2,1)S(1)} %multiply_convert_fusion.2), channel_id=1, source_target_pairs={{0,4},{4,8},{8,12},{12,16},{16,20},{20,24},{24,28},{28,32},{32,36}... | collective-permute-start | bytes 92168 | tf_op jit(solution)/shard_map/ppermute | solution.py:18
  52.1 0.6 copy-start.17
  62.7 86.5 %all-to-all-start = ((bf16[32,24,4096]{2,1,0:T(8,128)(2,1)}), bf16[32,24,4096]{2,1,0:T(8,128)(2,1)}, u32[]{:S(2)}, u32[]{:S(2)}) async-start(bf16[32,24,4096]{2,1,0:T(8,128)(2,1)} %bitcast.49), calls=%async_computation | async-start | bytes 12582912 | tf_op jit(solution)/shard_map/all_to_all | solution.py:412
  74.8 6.0 %copy-start.12 = (bf16[512,512]{1,0:T(8,128)(2,1)S(1)}, bf16[512,512]{1,0:T(8,128)(2,1)}, u32[]{:S(2)}) copy-start(bf16[512,512]{1,0:T(8,128)(2,1)} %param.18) | copy-start | bytes 1572868
  74.8 6.0 %copy-start.13 = (bf16[512,512]{1,0:T(8,128)(2,1)S(1)}, bf16[512,512]{1,0:T(8,128)(2,1)}, u32[]{:S(2)}) copy-start(bf16[512,512]{1,0:T(8,128)(2,1)} %param.17) | copy-start | bytes 1572868
  76.4 4.7 %copy-start.2 = (bf16[512,4096]{1,0:T(8,128)(2,1)S(1)}, bf16[512,4096]{1,0:T(8,128)(2,1)}, u32[]{:S(2)}) copy-start(bf16[512,4096]{1,0:T(8,128)(2,1)} %param.24) | copy-start | bytes 12582916
  76.4 70.9 %collective-permute-start.10 = (bf16[4096,256]{1,0:T(8,128)(2,1)}, bf16[4096,256]{1,0:T(8,128)(2,1)}, u32[]{:S(2)}, u32[]{:S(2)}) collective-permute-start(bf16[4096,256]{1,0:T(8,128)(2,1)} %pad_maximum_fusion.1), channel_id=1, source_target_pairs={{0,3},{1,2},{2,1},{3,0},{4,7},{5,6},{6,5},{7,4},{8,11},{9,10},{10,... | collective-permute-start | bytes 6291464 | tf_op jit(solution)/shard_map/ppermute | solution.py:22
  80.8 67.1 %collective-permute-start.9 = (bf16[4096,256]{1,0:T(8,128)(2,1)}, bf16[4096,256]{1,0:T(8,128)(2,1)}, u32[]{:S(2)}, u32[]{:S(2)}) collective-permute-start(bf16[4096,256]{1,0:T(8,128)(2,1)} %pad_maximum_fusion), channel_id=1, source_target_pairs={{0,1},{1,0},{2,3},{3,2},{4,5},{5,4},{6,7},{7,6},{8,9},{9,8},{10,11... | collective-permute-start | bytes 6291464 | tf_op jit(solution)/shard_map/ppermute | solution.py:22
  81.1 1.1 copy-start.19
  82.2 7.8 %copy-start.18 = (f32[4096]{0:T(1024)S(1)}, f32[4096]{0:T(1024)}, u32[]{:S(2)}) copy-start(f32[4096]{0:T(1024)} %param.25) | copy-start | bytes 49156
  87.9 40.9 %copy-start.23 = (bf16[4096,256]{1,0:T(8,128)(2,1)S(1)}, bf16[4096,256]{1,0:T(8,128)(2,1)}, u32[]{:S(2)}) copy-start(bf16[4096,256]{1,0:T(8,128)(2,1)} %param.32) | copy-start | bytes 6291460
  87.9 40.7 %collective-permute-start.2 = (f32[2,512]{1,0:T(2,128)S(1)}, f32[2,512]{1,0:T(2,128)S(1)}, u32[]{:S(2)}, u32[]{:S(2)}) collective-permute-start(f32[2,512]{1,0:T(2,128)S(1)} %pad_maximum_fusion.2), channel_id=1, source_target_pairs={{0,1},{1,0},{2,3},{3,2},{4,5},{5,4},{6,7},{7,6},{8,9},{9,8},{10,11... | collective-permute-start | bytes 12296 | tf_op jit(solution)/shard_map/ppermute | solution.py:22
  128.6 5.1 %collective-permute-start.3 = (f32[2,512]{1,0:T(2,128)S(1)}, f32[2,512]{1,0:T(2,128)S(1)}, u32[]{:S(2)}, u32[]{:S(2)}) collective-permute-start(f32[2,512]{1,0:T(2,128)S(1)} %pad_maximum_fusion.2), channel_id=1, source_target_pairs={{0,2},{1,3},{2,0},{3,1},{4,6},{5,7},{6,4},{7,5},{8,10},{9,11},{10,... | collective-permute-start | bytes 12296 | tf_op jit(solution)/shard_map/ppermute | solution.py:22
  133.7 5.6 %collective-permute-start.4 = (f32[2,512]{1,0:T(2,128)S(1)}, f32[2,512]{1,0:T(2,128)S(1)}, u32[]{:S(2)}, u32[]{:S(2)}) collective-permute-start(f32[2,512]{1,0:T(2,128)S(1)} %pad_maximum_fusion.2), channel_id=1, source_target_pairs={{0,3},{1,2},{2,1},{3,0},{4,7},{5,6},{6,5},{7,4},{8,11},{9,10},{10,... | collective-permute-start | bytes 12296 | tf_op jit(solution)/shard_map/ppermute | solution.py:22
  139.4 84.5 %collective-permute-start.16 = (bf16[256,2048]{1,0:T(8,128)(2,1)}, bf16[256,2048]{1,0:T(8,128)(2,1)}, u32[]{:S(2)}, u32[]{:S(2)}) collective-permute-start(bf16[256,2048]{1,0:T(8,128)(2,1)} %get-tuple-element.46), channel_id=1, source_target_pairs={{0,1},{1,0},{2,3},{3,2},{4,5},{5,4},{6,7},{7,6},{8,9},{9,8},{10,11... | collective-permute-start | bytes 3145736 | tf_op jit(solution)/shard_map/ppermute | solution.py:22
  139.4 87.2 %collective-permute-start.18 = (bf16[256,2048]{1,0:T(8,128)(2,1)}, bf16[256,2048]{1,0:T(8,128)(2,1)}, u32[]{:S(2)}, u32[]{:S(2)}) collective-permute-start(bf16[256,2048]{1,0:T(8,128)(2,1)} %get-tuple-element.48), channel_id=1, source_target_pairs={{0,3},{1,2},{2,1},{3,0},{4,7},{5,6},{6,5},{7,4},{8,11},{9,10},{10,... | collective-permute-start | bytes 3145736 | tf_op jit(solution)/shard_map/ppermute | solution.py:22
  143.5 44.5 %collective-permute-start.14 = (bf16[128,4096]{1,0:T(8,128)(2,1)S(1)}, bf16[128,4096]{1,0:T(8,128)(2,1)S(1)}, u32[]{:S(2)}, u32[]{:S(2)}) collective-permute-start(bf16[128,4096]{1,0:T(8,128)(2,1)S(1)} %slice.355), channel_id=1, source_target_pairs={{0,1},{1,0},{2,3},{3,2},{4,5},{5,4},{6,7},{7,6},{8,9},{9,8},{10,11... | collective-permute-start | bytes 3145736 | tf_op jit(solution)/shard_map/ppermute | solution.py:22
  147.3 46.9 %collective-permute-start.15 = (bf16[128,4096]{1,0:T(8,128)(2,1)}, bf16[128,4096]{1,0:T(8,128)(2,1)S(1)}, u32[]{:S(2)}, u32[]{:S(2)}) collective-permute-start(bf16[128,4096]{1,0:T(8,128)(2,1)} %slice.356), channel_id=1, source_target_pairs={{0,3},{1,2},{2,1},{3,0},{4,7},{5,6},{6,5},{7,4},{8,11},{9,10},{10,... | collective-permute-start | bytes 3145736 | tf_op jit(solution)/shard_map/ppermute | solution.py:22
  163.1 32.8 %collective-permute-start.11 = (bf16[384,512]{1,0:T(8,128)(2,1)}, bf16[384,512]{1,0:T(8,128)(2,1)}, u32[]{:S(2)}, u32[]{:S(2)}) collective-permute-start(bf16[384,512]{1,0:T(8,128)(2,1)} %get-tuple-element.44), channel_id=1, source_target_pairs={{0,2},{1,3},{2,0},{3,1},{4,6},{5,7},{6,4},{7,5},{8,10},{9,11},{10,... | collective-permute-start | bytes 1179656 | tf_op jit(solution)/shard_map/ppermute | solution.py:22
  188.1 7.8 %copy-start.3 = (bf16[128,4096]{1,0:T(8,128)(2,1)}, bf16[128,4096]{1,0:T(8,128)(2,1)S(1)}, u32[]{:S(2)}) copy-start(bf16[128,4096]{1,0:T(8,128)(2,1)S(1)} %collective-permute-done.14.refs_4_.refs_5_) | copy-start | bytes 3145732
  194.1 1.8 copy-start.4
  206.1 7.2 %copy-start.5 = (f32[512,512]{1,0:T(8,128)S(1)}, f32[512,512]{1,0:T(8,128)}, u32[]{:S(2)}) copy-start(f32[512,512]{1,0:T(8,128)} %get-tuple-element.58) | copy-start | bytes 3145732
  206.1 7.2 %copy-start.20 = (f32[512]{0:T(512)S(1)}, f32[512]{0:T(512)}, u32[]{:S(2)}) copy-start(f32[512]{0:T(512)} %param.22) | copy-start | bytes 6148
  206.1 7.2 %copy-start.21 = (f32[512]{0:T(512)S(1)}, f32[512]{0:T(512)}, u32[]{:S(2)}) copy-start(f32[512]{0:T(512)} %param.21) | copy-start | bytes 6148
  206.1 55.4 %all-to-all-start.1 = ((bf16[32,24,2048]{2,1,0:T(8,128)(2,1)}), bf16[32,24,2048]{2,1,0:T(8,128)(2,1)}, u32[]{:S(2)}, u32[]{:S(2)}) async-start(bf16[32,24,2048]{2,1,0:T(8,128)(2,1)} %bitcast.51), calls=%async_computation.1 | async-start | bytes 6291456 | tf_op jit(solution)/shard_map/all_to_all | solution.py:459
  214.6 9.3 %copy-start.6 = (bf16[256,2048]{1,0:T(8,128)(2,1)S(1)}, bf16[256,2048]{1,0:T(8,128)(2,1)}, u32[]{:S(2)}) copy-start(bf16[256,2048]{1,0:T(8,128)(2,1)} %get-tuple-element.45.refs_0_) | copy-start | bytes 3145732
  214.6 12.1 %copy-start.7 = (bf16[256,2048]{1,0:T(8,128)(2,1)S(1)}, bf16[256,2048]{1,0:T(8,128)(2,1)}, u32[]{:S(2)}) copy-start(bf16[256,2048]{1,0:T(8,128)(2,1)} %get-tuple-element.47.refs_3_) | copy-start | bytes 3145732
  221.1 27.5 %copy-start.9 = (bf16[256,2048]{1,0:T(8,128)(2,1)S(1)}, bf16[256,2048]{1,0:T(8,128)(2,1)}, u32[]{:S(2)}) copy-start(bf16[256,2048]{1,0:T(8,128)(2,1)} %get-tuple-element.52.refs_3_) | copy-start | bytes 3145732
  221.1 29.0 %copy-start.8 = (bf16[256,2048]{1,0:T(8,128)(2,1)S(1)}, bf16[256,2048]{1,0:T(8,128)(2,1)}, u32[]{:S(2)}) copy-start(bf16[256,2048]{1,0:T(8,128)(2,1)} %get-tuple-element.49.refs_0_) | copy-start | bytes 3145732
  221.1 27.5 %collective-permute-start.7 = (bf16[256,2048]{1,0:T(8,128)(2,1)}, bf16[256,2048]{1,0:T(8,128)(2,1)S(1)}, u32[]{:S(2)}, u32[]{:S(2)}) collective-permute-start(bf16[256,2048]{1,0:T(8,128)(2,1)} %get-tuple-element.40), channel_id=1, source_target_pairs={{0,3},{1,2},{2,1},{3,0},{4,7},{5,6},{6,5},{7,4},{8,11},{9,10},{10,... | collective-permute-start | bytes 3145736 | tf_op jit(solution)/shard_map/ppermute | solution.py:22
  223.9 26.2 %collective-permute-start.5 = (bf16[256,2048]{1,0:T(8,128)(2,1)}, bf16[256,2048]{1,0:T(8,128)(2,1)S(1)}, u32[]{:S(2)}, u32[]{:S(2)}) collective-permute-start(bf16[256,2048]{1,0:T(8,128)(2,1)} %get-tuple-element.38), channel_id=1, source_target_pairs={{0,1},{1,0},{2,3},{3,2},{4,5},{5,4},{6,7},{7,6},{8,9},{9,8},{10,11... | collective-permute-start | bytes 3145736 | tf_op jit(solution)/shard_map/ppermute | solution.py:22
  223.9 29.7 %copy-start.22 = (f32[128,2]{0,1:T(2,128)S(1)}, f32[128,2]{0,1:T(2,128)}, u32[]{:S(2)}) copy-start(f32[128,2]{0,1:T(2,128)} %param.27) | copy-start | bytes 3076
  225.9 33.9 %collective-permute-start.17 = (bf16[128,2048]{1,0:T(8,128)(2,1)}, bf16[128,2048]{1,0:T(8,128)(2,1)S(1)}, u32[]{:S(2)}, u32[]{:S(2)}) collective-permute-start(bf16[128,2048]{1,0:T(8,128)(2,1)} %add_convert_fusion.1), channel_id=1, source_target_pairs={{0,3},{1,2},{2,1},{3,0},{4,7},{5,6},{6,5},{7,4},{8,11},{9,10},{10,... | collective-permute-start | bytes 1572872 | tf_op jit(solution)/shard_map/ppermute | solution.py:22
  228.6 32.9 %collective-permute-start.19 = (bf16[128,2048]{1,0:T(8,128)(2,1)}, bf16[128,2048]{1,0:T(8,128)(2,1)}, u32[]{:S(2)}, u32[]{:S(2)}) collective-permute-start(bf16[128,2048]{1,0:T(8,128)(2,1)} %add_convert_fusion), channel_id=1, source_target_pairs={{0,1},{1,0},{2,3},{3,2},{4,5},{5,4},{6,7},{7,6},{8,9},{9,8},{10,11... | collective-permute-start | bytes 1572872 | tf_op jit(solution)/shard_map/ppermute | solution.py:22
  248.6 2.6 copy-start.10
  249.7 21.9 %collective-permute-start.8 = (bf16[128,2048]{1,0:T(8,128)(2,1)}, bf16[128,2048]{1,0:T(8,128)(2,1)S(1)}, u32[]{:S(2)}, u32[]{:S(2)}) collective-permute-start(bf16[128,2048]{1,0:T(8,128)(2,1)} %add_convert_fusion.2), channel_id=1, source_target_pairs={{0,1},{1,0},{2,3},{3,2},{4,5},{5,4},{6,7},{7,6},{8,9},{9,8},{10,11... | collective-permute-start | bytes 1572872 | tf_op jit(solution)/shard_map/ppermute | solution.py:22
  250.1 1.1 copy-start.11
  251.3 20.3 %collective-permute-start.6 = (bf16[128,2048]{1,0:T(8,128)(2,1)}, bf16[128,2048]{1,0:T(8,128)(2,1)}, u32[]{:S(2)}, u32[]{:S(2)}) collective-permute-start(bf16[128,2048]{1,0:T(8,128)(2,1)} %add_convert_fusion.3), channel_id=1, source_target_pairs={{0,3},{1,2},{2,1},{3,0},{4,7},{5,6},{6,5},{7,4},{8,11},{9,10},{10,... | collective-permute-start | bytes 1572872 | tf_op jit(solution)/shard_map/ppermute | solution.py:22
  259.8 1.7 copy-start.15
  261.5 14.8 %copy-start.1 = (bf16[4096,256]{1,0:T(8,128)(2,1)S(1)}, bf16[4096,256]{1,0:T(8,128)(2,1)}, u32[]{:S(2)}) copy-start(bf16[4096,256]{1,0:T(8,128)(2,1)} %param.31) | copy-start | bytes 6291460
  271.6 0.8 copy-start.16

commit v3 on v2

--- a/solution.py
+++ b/solution.py
@@ -26,10 +26,6 @@
     return jnp.dot(a, b, preferred_element_type=F32)
 
 
-def dot_rows(a, b):
-    return lax.dot_general(a, b, (((1,), (1,)), ((), ())), preferred_element_type=F32)
-
-
 def gated_product(gate, up):
     return (jax.nn.silu(gate) * up).astype(BF16)
 
@@ -46,18 +42,22 @@
     return (x * (65536 // by + 1)) >> 16
 
 
+def dot_columns(a, b):
+    return lax.dot_general(a, b, (((0,), (0,)), ((), ())), preferred_element_type=F32)
+
+
 def places(routes, experts):
-    rows = routes.shape[0]
-    expert = iota((rows, experts), 1)
-    named = (routes[:, 0:1] == expert) | (routes[:, 1:2] == expert)
-    earlier = ones_where(iota((rows, rows), 1) < iota((rows, rows), 0))
-    return jnp.where(named, dot(earlier, ones_where(named)), -1.0)
+    rows = routes.shape[1]
+    expert = iota((experts, rows), 0)
+    named = (routes[0:1, :] == expert) | (routes[1:2, :] == expert)
+    earlier = ones_where(iota((rows, rows), 0) < iota((rows, rows), 1))
+    return jnp.where(named, dot(ones_where(named), earlier), -1.0)
 
 
 def outbox_body(flags, tokens, gain, own, other, out, rows, place, select, *, capacity, chunk):
     step = pl.program_id(0)
-    block, width = own.shape[0], gain.shape[1]
-    experts = place.shape[1]
+    block, width = own.shape[1], gain.shape[1]
+    experts = place.shape[0]
 
     @pl.when(step == 0)
     def _():
@@ -68,17 +68,17 @@
             rows[pl.ds(pl.multiple_of(i * chunk, chunk), chunk), :] = (x * scale * gain[...]).astype(BF16)
             return carry
 
-        lax.fori_loop(0, 2 * block // chunk, norm, 0)
+        lax.fori_loop(0, 2 * block // chunk, norm, 0, unroll=2)
         first = flags[1] == 0
-        place[:block, :] = places(jnp.where(first, own[...], other[...]), experts).astype(BF16)
-        place[block:, :] = places(jnp.where(first, other[...], own[...]), experts).astype(BF16)
+        place[:, :block] = places(jnp.where(first, own[...], other[...]), experts).astype(BF16)
+        place[:, block:] = places(jnp.where(first, other[...], own[...]), experts).astype(BF16)
         slots = select.shape[0]
         slot = iota((slots, 1), 0)
         expert = quotient(slot, 2 * capacity)
         within = slot - expert * (2 * capacity)
         second = jnp.where(within >= capacity, 1, 0)
         wanted = (within - second * capacity).astype(F32)
-        there = dot_rows(ones_where(expert == iota((slots, experts), 1)), place[...])
+        there = dot(ones_where(expert == iota((slots, experts), 1)), place[...])
         row_block = jnp.where(iota((slots, 2 * block), 1) >= block, 1, 0)
         select[...] = ones_where((there == wanted) & (row_block == second))
 
@@ -89,7 +89,7 @@
 
 def outbox_of(flags, tokens, gain, own, other, experts, capacity):
     width = tokens.shape[1]
-    block = own.shape[0]
+    block = own.shape[1]
     slots = experts * 2 * capacity
     here = 512
     return pl.pallas_call(
@@ -106,7 +106,7 @@
             out_specs=pl.BlockSpec((slots, here), lambda i, f: (0, i)),
             scratch_shapes=[
                 pltpu.VMEM((2 * block, width), BF16),
-                pltpu.VMEM((2 * block, experts), BF16),
+                pltpu.VMEM((experts, 2 * block), BF16),
                 pltpu.VMEM((slots, 2 * block), BF16),
             ],
         ),
@@ -256,11 +256,11 @@
 
 
 def portions_body(routes, weights, mix, *, capacity, experts):
-    block, slots = routes.shape[0], mix.shape[2]
+    block, slots = routes.shape[1], mix.shape[1]
     chosen = routes[...]
-    expert = iota((block, experts), 1)
-    weight = jnp.where(chosen[:, 0:1] == expert, weights[:, 0:1], 0.0) + jnp.where(
-        chosen[:, 1:2] == expert, weights[:, 1:2], 0.0
+    expert = iota((experts, block), 0)
+    weight = jnp.where(chosen[0:1, :] == expert, weights[0:1, :], 0.0) + jnp.where(
+        chosen[1:2, :] == expert, weights[1:2, :], 0.0
     )
     upper = weight.astype(BF16)
     lower = (weight - upper.astype(F32)).astype(BF16)
@@ -270,20 +270,19 @@
     within = lane - quotient(lane, 2 * capacity) * (2 * capacity)
     second = jnp.where(within >= capacity, 1, 0)
     wanted = (within - second * capacity).astype(F32)
-    hit = dot(places(chosen, experts).astype(BF16), unfold) == wanted
+    hit = dot_columns(places(chosen, experts).astype(BF16), unfold) == wanted
     for part, values in enumerate((upper, lower)):
-        there = dot(values, unfold)
+        there = dot_columns(values, unfold)
         for side in range(2):
-            mix[side, part * block : (part + 1) * block, :] = jnp.where(
-                hit & (second == side), there, 0.0
-            ).astype(BF16)
+            at = (2 * side + part) * block
+            mix[at : at + block, :] = jnp.where(hit & (second == side), there, 0.0).astype(BF16)
 
 
 def portions_of(routes, weights, experts, capacity):
-    block, slots = routes.shape[0], 2 * experts * capacity
+    block, slots = routes.shape[1], 2 * experts * capacity
     return pl.pallas_call(
         partial(portions_body, capacity=capacity, experts=experts),
-        out_shape=jax.ShapeDtypeStruct((2, 2 * block, slots), BF16),
+        out_shape=jax.ShapeDtypeStruct((4 * block, slots), BF16),
         cost_estimate=pl.CostEstimate(flops=6 * block * slots * experts, bytes_accessed=8 * block * slots, transcendentals=0),
         name="portions",
     )(routes, weights)
@@ -304,10 +303,9 @@
 
 def mixed_of(portions, returned, shared):
     slots, width = returned.shape
-    block = portions.shape[1] // 2
+    block = portions.shape[0] // 4
     step = 512
     count = width // step
-    portions = portions.reshape(4 * block, slots)
     return pl.pallas_call(
         mix_body,
         grid=(count,),
@@ -321,28 +319,6 @@
         cost_estimate=pl.CostEstimate(flops=8 * block * slots * width, bytes_accessed=2 * width * (slots + 8 * block), transcendentals=0),
         name="mix",
     )(portions, returned, *shared)
-
-
-def sum_body(*refs):
-    parts, out = refs[:-1], refs[-1]
-    width = out.shape[1] // 2
-    for side in range(2):
-        total = sum(part[...].astype(F32) for part in parts[3 * side : 3 * side + 3])
-        out[:, side * width : (side + 1) * width] = total.astype(BF16)
-
-
-def sum_of(parts):
-    block, width = parts[2].shape
-    rows = 32
-    return pl.pallas_call(
-        sum_body,
-        grid=(block // rows,),
-        in_specs=[pl.BlockSpec((rows, width), lambda i: (i, 0))] * 6,
-        out_specs=pl.BlockSpec((rows, 2 * width), lambda i: (i, 0)),
-        out_shape=jax.ShapeDtypeStruct((block, 2 * width), BF16),
-        cost_estimate=pl.CostEstimate(flops=4 * block * width, bytes_accessed=16 * block * width, transcendentals=0),
-        name="sum",
-    )(*parts)
 
 
 def gated_of(value_in, gate_in):
@@ -399,6 +375,7 @@
     half = gate_local.shape[1] // 2
     down_half = down_local.shape[0] // 2
 
+    routes = routes.T
     other_routes = swapped(routes, "tp", 2)
 
     rim = value_in.shape[0] - (conv_taps.shape[0] - 1)
@@ -459,10 +436,12 @@
     returned = lax.all_to_all(
         expert_rows.reshape(ep_count, 2 * capacity, width // 2), "ep", split_axis=0, concat_axis=0, tiled=True
     ).reshape(2 * capacity * ep_count, width // 2)
-    portions = portions_of(routes, route_weights, ep_count, capacity)
+    portions = portions_of(routes, route_weights.T, ep_count, capacity)
     experts_out = mixed_of(portions, returned, shared_sums)
-    *mixer_sums, experts_out = lax.optimization_barrier((*mixer_sums, experts_out))
-    mixer_rows = sum_of(mixer_sums)
+    own = [mixer_sums[i][:rows_own].astype(F32) + mixer_sums[i + 1][:rows_own].astype(F32) for i in (0, 3)]
+    own = jnp.concatenate(own, axis=1)
+    own, left_2, right_2, experts_out = lax.optimization_barrier((own, mixer_sums[2], mixer_sums[5], experts_out))
+    mixer_rows = (own + jnp.concatenate([left_2, right_2], axis=1).astype(F32)).astype(BF16)
     return (mixer_rows, experts_out)
 
 

time: 278 us -> 275 us (0.989)
  Pallas kernels: 58.4 us -> 54 us
  other arithmetic: 19.1 us -> 22.8 us
    pallas_call x1 -> x0, Pallas kernels: 3.96 us -> none  [sum_of(): pl.pallas_call(sum_body, grid=(block // rows,), in_specs=[pl.BlockSpec((r...]
    convert_element_type x0 -> x1, other arithmetic: none -> 3.01 us  [per_device(): (own + jnp.concatenate([left_2, right_2], axis=1).astype(F32)).astype(BF16)]
  transfers between devices with their start and end apart: 22 -> 22, of which waited for: 12 -> 10; matrix products, arithmetic and copies ran while one was open for 12% -> 12% of each run, Pallas kernels for 20% -> 20%
where the time goes in v3:
time: 275 us; the launch traced here: 273 us
  waiting for transfers between devices  140 us (51%)
  Pallas kernels  54 us (20%)
  starting transfers between devices  39.2 us (14%)
  other arithmetic  22.8 us (8%)
  local copies, waits for them, and re-layouts  12.6 us (5%)
  matrix products  3.47 us (1%)
    ppermute x19, waiting for transfers between devices, swapped(): lax.ppermute(x, axis, [(i, i ^ bits) for i in range(lax.axis_size(axis))])  139 us
    ppermute x19, starting transfers between devices, swapped(): lax.ppermute(x, axis, [(i, i ^ bits) for i in range(lax.axis_size(axis))])  22.4 us
    pallas_call x1, Pallas kernels, hidden_of(): pl.pallas_call(partial(hidden_body, capacity=capacity, chunk=64), grid_sp...  14 us
    pallas_call x2, Pallas kernels, halves_of(): pl.pallas_call(halves_body, grid_spec=pltpu.PrefetchScalarGridSpec(num_sc...  11.7 us
    pallas_call x1, Pallas kernels, down_of(): pl.pallas_call(partial(down_body, capacity=capacity), grid=(count,), in_s...  10.2 us
    pallas_call x1, Pallas kernels, outbox_of(): pl.pallas_call(partial(outbox_body, capacity=capacity, chunk=32), grid_sp...  9.5 us
    all_to_all x1, starting transfers between devices, per_device(): lax.all_to_all(outbox.reshape(ep_count, 2 * capacity, width), 'ep', split...  8.55 us
    all_to_all x1, starting transfers between devices, per_device(): lax.all_to_all(expert_rows.reshape(ep_count, 2 * capacity, width // 2), '...  7.03 us
  transfers between devices with their start and end apart: 22, of which 10 were waited for; matrix products, arithmetic and copies ran while one was open for 12% of the time, Pallas kernels for 20%

profile of v3, /device:TPU:0, one launch (start us, length us, event | category | flops | bytes accessed | tf_op | source)
XLA Modules:
  0.0 273.4 jit_solution(16116056851841522064)
XLA Ops:
  0.6 2.9 %collective-permute-start.13 = (bf16[256,4096]{1,0:T(8,128)(2,1)}, bf16[256,4096]{1,0:T(8,128)(2,1)}, u32[]{:S(2)}, u32[]{:S(2)}) collective-permute-start(bf16[256,4096]{1,0:T(8,128)(2,1)} %bitcast.53), channel_id=1, source_target_pairs={{0,3},{1,2},{2,1},{3,0},{4,7},{5,6},{6,5},{7,4},{8,11},{9,10},{10,... | collective-permute-start | bytes 6291464 | tf_op jit(solution)/shard_map/ppermute | solution.py:22
  3.8 1.6 collective-permute-start.1
  6.2 1.3 collective-permute-start
  7.5 1.1 fusion.44
  8.7 1.1 fusion.45
  10.4 40.3 %collective-permute-done.1.other = s32[2,128]{1,0:T(2,128)S(1)} collective-permute-done((s32[2,128]{1,0:T(2,128)}, s32[2,128]{1,0:T(2,128)S(1)}, u32[]{:S(2)}, u32[]{:S(2)}) %collective-permute-start.1) | collective-permute-done | bytes 1056 | tf_op jit(solution)/shard_map/ppermute | solution.py:22
  51.3 9.5 %outbox.1 = bf16[768,4096]{1,0:T(8,128)(2,1)} custom-call(s32[2]{0:T(128)} %pad_add_fusion.flags, bf16[2,2,128,4096]{3,2,1,0:T(8,128)(2,1)} %bitcast.51, f32[1,4096]{1,0:T(1,128)} %bitcast.67, s32[2,128]{1,0:T(2,128)} %bitcast.101, s32[2,128]{1,0:T(2,128)} %copy-done.18), custom_call_target="tpu_custom_call" | custom-call | flops 1610612736 | bytes 8388608 | tf_op jit(solution)/shard_map/outbox/pallas_call | solution.py:95
  60.8 8.5 %all-to-all-start = ((bf16[32,24,4096]{2,1,0:T(8,128)(2,1)}), bf16[32,24,4096]{2,1,0:T(8,128)(2,1)}, u32[]{:S(2)}, u32[]{:S(2)}) async-start(bf16[32,24,4096]{2,1,0:T(8,128)(2,1)} %bitcast.50), calls=%async_computation | async-start | bytes 12582912 | tf_op jit(solution)/shard_map/all_to_all | solution.py:389
  69.4 2.4 fusion.42
  71.8 1.6 pad_maximum_fusion.2
  73.4 2.8 %collective-permute-start.10 = (bf16[4096,256]{1,0:T(8,128)(2,1)}, bf16[4096,256]{1,0:T(8,128)(2,1)}, u32[]{:S(2)}, u32[]{:S(2)}) collective-permute-start(bf16[4096,256]{1,0:T(8,128)(2,1)} %pad_maximum_fusion.2), channel_id=1, source_target_pairs={{0,3},{1,2},{2,1},{3,0},{4,7},{5,6},{6,5},{7,4},{8,11},{9,10},{10,... | collective-permute-start | bytes 6291464 | tf_op jit(solution)/shard_map/ppermute | solution.py:22
  76.2 1.6 pad_maximum_fusion.1
  78.1 1.0 copy-done.2
  80.2 5.0 %fusion.40 = (f32[512]{0:T(512)S(1)}, f32[512]{0:T(512)S(1)}, f32[512,512]{1,0:T(8,128)S(1)}) fusion(f32[542,512]{1,0:T(8,128)S(1)} %maximum_convert_fusion, f32[512]{0:T(512)S(1)} %bitcast.97, f32[512]{0:T(512)S(1)} %bitcast.98, f32[512]{0:T(512)S(1)} %bitcast.69, f32[512]{0:T(512)S(1)} %bitcast.70, f32[512]{0:T(512)S(1)} %bitcast.71, f32[512]{0:T(512)S(1)} %bitcast.72, ...), kind=kLoop, calls=%fused_computation.92 | loop fusion | flops 17038336 | bytes 33624064 | tf_op jit(solution)/shard_map/reduce_sum | solution.py:404
  85.3 1.1 collective-permute-start.2
  86.4 1.4 fusion.4
  87.7 37.9 %collective-permute-done.2 = f32[2,512]{1,0:T(2,128)S(1)} collective-permute-done((f32[2,512]{1,0:T(2,128)S(1)}, f32[2,512]{1,0:T(2,128)S(1)}, u32[]{:S(2)}, u32[]{:S(2)}) %collective-permute-start.2) | collective-permute-done | bytes 4128 | tf_op jit(solution)/shard_map/ppermute | solution.py:22
  125.8 2.1 fusion.6.hidden
  127.9 2.8 %collective-permute-done.3 = f32[2,512]{1,0:T(2,128)S(1)} collective-permute-done((f32[2,512]{1,0:T(2,128)S(1)}, f32[2,512]{1,0:T(2,128)S(1)}, u32[]{:S(2)}, u32[]{:S(2)}) %collective-permute-start.3) | collective-permute-done | bytes 4128 | tf_op jit(solution)/shard_map/ppermute | solution.py:22
  131.2 5.1 %shard_map.176 = (bf16[256,2048]{1,0:T(8,128)(2,1)}, bf16[256,2048]{1,0:T(8,128)(2,1)}, bf16[256,2048]{1,0:T(8,128)(2,1)}, bf16[256,2048]{1,0:T(8,128)(2,1)}) custom-call(s32[2]{0:T(128)} %pad_add_fusion.flags, bf16[512,256]{1,0:T(8,128)(2,1)} %fusion.6.hidden, bf16[256,4096]{1,0:T(8,128)(2,1)} %down.3), custom_call_target="tpu_custom_call" | custom-call | flops 1073741824 | bytes 6291456 | tf_op jit(solution)/shard_map/pallas_call | solution.py:245
  136.4 2.8 %collective-permute-start.18 = (bf16[256,2048]{1,0:T(8,128)(2,1)}, bf16[256,2048]{1,0:T(8,128)(2,1)}, u32[]{:S(2)}, u32[]{:S(2)}) collective-permute-start(bf16[256,2048]{1,0:T(8,128)(2,1)} %get-tuple-element.45), channel_id=1, source_target_pairs={{0,3},{1,2},{2,1},{3,0},{4,7},{5,6},{6,5},{7,4},{8,11},{9,10},{10,... | collective-permute-start | bytes 3145736 | tf_op jit(solution)/shard_map/ppermute | solution.py:22
  139.3 2.3 slice.373
  141.5 1.4 collective-permute-start.14
  143.0 2.3 slice.374
  145.9 1.4 all-to-all-done
  147.2 14.0 %hidden.1 = (bf16[384,512]{1,0:T(8,128)(2,1)}, bf16[384,512]{1,0:T(8,128)(2,1)}) custom-call(s32[2]{0:T(128)} %pad_add_fusion.flags, bf16[768,4096]{1,0:T(8,128)(2,1)} %bitcast.44.arrived, bf16[4096,256]{1,0:T(8,128)(2,1)} %bitcast.58, bf16[4096,256]{1,0:T(8,128)(2,1)} %bitcast.60, bf16[4096,256]{1,0:T(8,128)(2,1)} %collective-permute-done.9.first, ...), custom_call_target="tpu_custom_call" | custom-call | flops 6442450944 | bytes 14680064 | tf_op jit(solution)/shard_map/hidden/pallas_call | solution.py:162
  161.3 1.9 collective-permute-start.11
  163.2 21.9 %collective-permute-done.14.refs_4_.refs_5_ = bf16[128,4096]{1,0:T(8,128)(2,1)S(1)} collective-permute-done((bf16[128,4096]{1,0:T(8,128)(2,1)}, bf16[128,4096]{1,0:T(8,128)(2,1)S(1)}, u32[]{:S(2)}, u32[]{:S(2)}) %collective-permute-start.14) | collective-permute-done | bytes 1048608 | tf_op jit(solution)/shard_map/ppermute | solution.py:22
  185.1 6.1 %collective-permute-done.15.refs_6_.refs_7_ = bf16[128,4096]{1,0:T(8,128)(2,1)S(1)} collective-permute-done((bf16[128,4096]{1,0:T(8,128)(2,1)}, bf16[128,4096]{1,0:T(8,128)(2,1)S(1)}, u32[]{:S(2)}, u32[]{:S(2)}) %collective-permute-start.15) | collective-permute-done | bytes 1048608 | tf_op jit(solution)/shard_map/ppermute | solution.py:22
  191.2 1.7 collective-permute-done.11.got
  193.6 10.2 %down.5 = bf16[768,2048]{1,0:T(8,128)(2,1)} custom-call(bf16[384,512]{1,0:T(8,128)(2,1)} %get-tuple-element.40.kept, bf16[384,512]{1,0:T(8,128)(2,1)} %copy-done.13, bf16[256,4096]{1,0:T(8,128)(2,1)} %bitcast.55, bf16[256,4096]{1,0:T(8,128)(2,1)} %bitcast.56, bf16[256,4096]{1,0:T(8,128)(2,1)} %collective-permute-done.12.refs_2_.refs_3_, ...), custom_call_target="tpu_custom_call" | custom-call | flops 3221225472 | bytes 11534336 | tf_op jit(solution)/shard_map/down/pallas_call | solution.py:213
  203.8 7.0 %all-to-all-start.1 = ((bf16[32,24,2048]{2,1,0:T(8,128)(2,1)}), bf16[32,24,2048]{2,1,0:T(8,128)(2,1)}, u32[]{:S(2)}, u32[]{:S(2)}) async-start(bf16[32,24,2048]{2,1,0:T(8,128)(2,1)} %bitcast.52), calls=%async_computation.1 | async-start | bytes 6291456 | tf_op jit(solution)/shard_map/all_to_all | solution.py:436
  210.8 1.3 multiply_convert_fusion.hidden
  212.1 6.6 %shard_map.177 = (bf16[256,2048]{1,0:T(8,128)(2,1)}, bf16[256,2048]{1,0:T(8,128)(2,1)}, bf16[256,2048]{1,0:T(8,128)(2,1)}, bf16[256,2048]{1,0:T(8,128)(2,1)}) custom-call(s32[2]{0:T(128)} %pad_add_fusion.flags, bf16[512,512]{1,0:T(8,128)(2,1)} %multiply_convert_fusion.hidden, bf16[512,4096]{1,0:T(8,128)(2,1)} %down.4), custom_call_target="tpu_custom_call" | custom-call | flops 2147483648 | bytes 8388608 | tf_op jit(solution)/shard_map/pallas_call | solution.py:245
  219.1 2.4 portions.1
  221.4 2.2 collective-permute-start.6
  223.7 1.2 add_convert_fusion.2
  224.9 1.1 collective-permute-start.17
  225.9 1.2 add_convert_fusion.1
  227.4 17.6 %collective-permute-done.5 = bf16[256,2048]{1,0:T(8,128)(2,1)} collective-permute-done((bf16[256,2048]{1,0:T(8,128)(2,1)}, bf16[256,2048]{1,0:T(8,128)(2,1)}, u32[]{:S(2)}, u32[]{:S(2)}) %collective-permute-start.5) | collective-permute-done | bytes 1048608 | tf_op jit(solution)/shard_map/ppermute | solution.py:22
  245.0 2.4 add_convert_fusion.4
  247.4 2.2 collective-permute-start.7
  249.6 1.2 add_convert_fusion.3
  250.8 1.6 pad_maximum_fusion
  252.4 7.7 %collective-permute-done.17.refs_2_ = bf16[128,2048]{1,0:T(8,128)(2,1)S(1)} collective-permute-done((bf16[128,2048]{1,0:T(8,128)(2,1)S(1)}, bf16[128,2048]{1,0:T(8,128)(2,1)S(1)}, u32[]{:S(2)}, u32[]{:S(2)}) %collective-permute-start.17) | collective-permute-done | bytes 524320 | tf_op jit(solution)/shard_map/ppermute | solution.py:22
  261.1 6.3 %mix.1 = bf16[128,4096]{1,0:T(8,128)(2,1)} custom-call(bf16[512,768]{1,0:T(8,128)(2,1)} %portions.1, bf16[768,2048]{1,0:T(8,128)(2,1)} %bitcast.47.returned, bf16[256,2048]{1,0:T(8,128)(2,1)} %get-tuple-element.42.refs_0_, bf16[256,2048]{1,0:T(8,128)(2,1)} %collective-permute-done.16.refs_1_, bf16[128,2048]{1,0:T(8,128)(2,1)} %copy-done.11, ...), custom_call_target="tpu_custom_call" | custom-call | flops 1610612736 | bytes 7340032 | tf_op jit(solution)/shard_map/mix/pallas_call | solution.py:309
  267.4 3.0 %collective-permute-done.7 = bf16[128,2048]{1,0:T(8,128)(2,1)} collective-permute-done((bf16[128,2048]{1,0:T(8,128)(2,1)}, bf16[128,2048]{1,0:T(8,128)(2,1)}, u32[]{:S(2)}, u32[]{:S(2)}) %collective-permute-start.7) | collective-permute-done | bytes 524320 | tf_op jit(solution)/shard_map/ppermute | solution.py:22
  270.4 3.0 %add_convert_fusion = bf16[128,4096]{1,0:T(8,128)(2,1)} fusion(f32[128,4096]{1,0:T(8,128)} %pad_maximum_fusion, bf16[128,2048]{1,0:T(8,128)(2,1)} %collective-permute-done.8, bf16[128,2048]{1,0:T(8,128)(2,1)} %collective-permute-done.7), kind=kLoop, calls=%fused_computation.8 | loop fusion | flops 3145728 | bytes 4194304 | tf_op jit(solution)/shard_map/convert_element_type | solution.py:444
  (70 shorter events, 7.4 us)
Async XLA Ops:
  0.6 85.7 %copy-start = (bf16[4096,256]{1,0:T(8,128)(2,1)S(1)}, bf16[4096,256]{1,0:T(8,128)(2,1)}, u32[]{:S(2)}) copy-start(bf16[4096,256]{1,0:T(8,128)(2,1)} %param.31) | copy-start | bytes 6291460
  0.6 135.8 %collective-permute-start.13 = (bf16[256,4096]{1,0:T(8,128)(2,1)}, bf16[256,4096]{1,0:T(8,128)(2,1)}, u32[]{:S(2)}, u32[]{:S(2)}) collective-permute-start(bf16[256,4096]{1,0:T(8,128)(2,1)} %bitcast.53), channel_id=1, source_target_pairs={{0,3},{1,2},{2,1},{3,0},{4,7},{5,6},{6,5},{7,4},{8,11},{9,10},{10,... | collective-permute-start | bytes 6291464 | tf_op jit(solution)/shard_map/ppermute | solution.py:22
  3.6 137.9 %collective-permute-start.12 = (bf16[256,4096]{1,0:T(8,128)(2,1)}, bf16[256,4096]{1,0:T(8,128)(2,1)}, u32[]{:S(2)}, u32[]{:S(2)}) collective-permute-start(bf16[256,4096]{1,0:T(8,128)(2,1)} %bitcast.54), channel_id=1, source_target_pairs={{0,1},{1,0},{2,3},{3,2},{4,5},{5,4},{6,7},{7,6},{8,9},{9,8},{10,11... | collective-permute-start | bytes 6291464 | tf_op jit(solution)/shard_map/ppermute | solution.py:22
  3.8 46.9 %collective-permute-start.1 = (s32[2,128]{1,0:T(2,128)}, s32[2,128]{1,0:T(2,128)S(1)}, u32[]{:S(2)}, u32[]{:S(2)}) collective-permute-start(s32[2,128]{1,0:T(2,128)} %bitcast.100), channel_id=1, source_target_pairs={{0,2},{1,3},{2,0},{3,1},{4,6},{5,7},{6,4},{7,5},{8,10},{9,11},{10,... | collective-permute-start | bytes 3080 | tf_op jit(solution)/shard_map/ppermute | solution.py:22
  6.2 73.8 %collective-permute-start = (bf16[30,512]{1,0:T(8,128)(2,1)S(1)}, bf16[30,512]{1,0:T(8,128)(2,1)S(1)}, u32[]{:S(2)}, u32[]{:S(2)}) collective-permute-start(bf16[30,512]{1,0:T(8,128)(2,1)S(1)} %multiply_convert_fusion.2), channel_id=1, source_target_pairs={{0,4},{4,8},{8,12},{12,16},{16,20},{20,24},{24,28},{28,32},{32,36}... | collective-permute-start | bytes 92168 | tf_op jit(solution)/shard_map/ppermute | solution.py:18
  50.7 0.6 copy-start.18
  60.8 86.4 %all-to-all-start = ((bf16[32,24,4096]{2,1,0:T(8,128)(2,1)}), bf16[32,24,4096]{2,1,0:T(8,128)(2,1)}, u32[]{:S(2)}, u32[]{:S(2)}) async-start(bf16[32,24,4096]{2,1,0:T(8,128)(2,1)} %bitcast.50), calls=%async_computation | async-start | bytes 12582912 | tf_op jit(solution)/shard_map/all_to_all | solution.py:389
  71.8 6.0 %copy-start.9 = (bf16[512,512]{1,0:T(8,128)(2,1)S(1)}, bf16[512,512]{1,0:T(8,128)(2,1)}, u32[]{:S(2)}) copy-start(bf16[512,512]{1,0:T(8,128)(2,1)} %param.18) | copy-start | bytes 1572868
  71.8 6.0 %copy-start.10 = (bf16[512,512]{1,0:T(8,128)(2,1)S(1)}, bf16[512,512]{1,0:T(8,128)(2,1)}, u32[]{:S(2)}) copy-start(bf16[512,512]{1,0:T(8,128)(2,1)} %param.17) | copy-start | bytes 1572868
  73.4 71.8 %collective-permute-start.10 = (bf16[4096,256]{1,0:T(8,128)(2,1)}, bf16[4096,256]{1,0:T(8,128)(2,1)}, u32[]{:S(2)}, u32[]{:S(2)}) collective-permute-start(bf16[4096,256]{1,0:T(8,128)(2,1)} %pad_maximum_fusion.2), channel_id=1, source_target_pairs={{0,3},{1,2},{2,1},{3,0},{4,7},{5,6},{6,5},{7,4},{8,11},{9,10},{10,... | collective-permute-start | bytes 6291464 | tf_op jit(solution)/shard_map/ppermute | solution.py:22
  76.2 2.9 %copy-start.2 = (bf16[512,4096]{1,0:T(8,128)(2,1)S(1)}, bf16[512,4096]{1,0:T(8,128)(2,1)}, u32[]{:S(2)}) copy-start(bf16[512,4096]{1,0:T(8,128)(2,1)} %param.24) | copy-start | bytes 12582916
  77.8 68.0 %collective-permute-start.9 = (bf16[4096,256]{1,0:T(8,128)(2,1)}, bf16[4096,256]{1,0:T(8,128)(2,1)}, u32[]{:S(2)}, u32[]{:S(2)}) collective-permute-start(bf16[4096,256]{1,0:T(8,128)(2,1)} %pad_maximum_fusion.1), channel_id=1, source_target_pairs={{0,1},{1,0},{2,3},{3,2},{4,5},{5,4},{6,7},{7,6},{8,9},{9,8},{10,11... | collective-permute-start | bytes 6291464 | tf_op jit(solution)/shard_map/ppermute | solution.py:22
  79.1 1.1 copy-start.15
  80.2 6.1 %copy-start.14 = (f32[4096]{0:T(1024)S(1)}, f32[4096]{0:T(1024)}, u32[]{:S(2)}) copy-start(f32[4096]{0:T(1024)} %param.25) | copy-start | bytes 49156
  85.2 40.6 %copy-start.19 = (bf16[4096,256]{1,0:T(8,128)(2,1)S(1)}, bf16[4096,256]{1,0:T(8,128)(2,1)}, u32[]{:S(2)}) copy-start(bf16[4096,256]{1,0:T(8,128)(2,1)} %param.32) | copy-start | bytes 6291460
  85.3 40.4 %collective-permute-start.2 = (f32[2,512]{1,0:T(2,128)S(1)}, f32[2,512]{1,0:T(2,128)S(1)}, u32[]{:S(2)}, u32[]{:S(2)}) collective-permute-start(f32[2,512]{1,0:T(2,128)S(1)} %pad_maximum_fusion.3), channel_id=1, source_target_pairs={{0,1},{1,0},{2,3},{3,2},{4,5},{5,4},{6,7},{7,6},{8,9},{9,8},{10,11... | collective-permute-start | bytes 12296 | tf_op jit(solution)/shard_map/ppermute | solution.py:22
  125.7 5.1 %collective-permute-start.3 = (f32[2,512]{1,0:T(2,128)S(1)}, f32[2,512]{1,0:T(2,128)S(1)}, u32[]{:S(2)}, u32[]{:S(2)}) collective-permute-start(f32[2,512]{1,0:T(2,128)S(1)} %pad_maximum_fusion.3), channel_id=1, source_target_pairs={{0,2},{1,3},{2,0},{3,1},{4,6},{5,7},{6,4},{7,5},{8,10},{9,11},{10,... | collective-permute-start | bytes 12296 | tf_op jit(solution)/shard_map/ppermute | solution.py:22
  130.8 5.6 %collective-permute-start.4 = (f32[2,512]{1,0:T(2,128)S(1)}, f32[2,512]{1,0:T(2,128)S(1)}, u32[]{:S(2)}, u32[]{:S(2)}) collective-permute-start(f32[2,512]{1,0:T(2,128)S(1)} %pad_maximum_fusion.3), channel_id=1, source_target_pairs={{0,3},{1,2},{2,1},{3,0},{4,7},{5,6},{6,5},{7,4},{8,11},{9,10},{10,... | collective-permute-start | bytes 12296 | tf_op jit(solution)/shard_map/ppermute | solution.py:22
  136.4 87.3 %collective-permute-start.16 = (bf16[256,2048]{1,0:T(8,128)(2,1)}, bf16[256,2048]{1,0:T(8,128)(2,1)}, u32[]{:S(2)}, u32[]{:S(2)}) collective-permute-start(bf16[256,2048]{1,0:T(8,128)(2,1)} %get-tuple-element.43), channel_id=1, source_target_pairs={{0,1},{1,0},{2,3},{3,2},{4,5},{5,4},{6,7},{7,6},{8,9},{9,8},{10,11... | collective-permute-start | bytes 3145736 | tf_op jit(solution)/shard_map/ppermute | solution.py:22
  136.4 89.5 %collective-permute-start.18 = (bf16[256,2048]{1,0:T(8,128)(2,1)}, bf16[256,2048]{1,0:T(8,128)(2,1)}, u32[]{:S(2)}, u32[]{:S(2)}) collective-permute-start(bf16[256,2048]{1,0:T(8,128)(2,1)} %get-tuple-element.45), channel_id=1, source_target_pairs={{0,3},{1,2},{2,1},{3,0},{4,7},{5,6},{6,5},{7,4},{8,11},{9,10},{10,... | collective-permute-start | bytes 3145736 | tf_op jit(solution)/shard_map/ppermute | solution.py:22
  141.5 43.5 %collective-permute-start.14 = (bf16[128,4096]{1,0:T(8,128)(2,1)}, bf16[128,4096]{1,0:T(8,128)(2,1)S(1)}, u32[]{:S(2)}, u32[]{:S(2)}) collective-permute-start(bf16[128,4096]{1,0:T(8,128)(2,1)} %slice.373), channel_id=1, source_target_pairs={{0,1},{1,0},{2,3},{3,2},{4,5},{5,4},{6,7},{7,6},{8,9},{9,8},{10,11... | collective-permute-start | bytes 3145736 | tf_op jit(solution)/shard_map/ppermute | solution.py:22
  145.2 45.9 %collective-permute-start.15 = (bf16[128,4096]{1,0:T(8,128)(2,1)}, bf16[128,4096]{1,0:T(8,128)(2,1)S(1)}, u32[]{:S(2)}, u32[]{:S(2)}) collective-permute-start(bf16[128,4096]{1,0:T(8,128)(2,1)} %slice.374), channel_id=1, source_target_pairs={{0,3},{1,2},{2,1},{3,0},{4,7},{5,6},{6,5},{7,4},{8,11},{9,10},{10,... | collective-permute-start | bytes 3145736 | tf_op jit(solution)/shard_map/ppermute | solution.py:22
  161.3 31.6 %collective-permute-start.11 = (bf16[384,512]{1,0:T(8,128)(2,1)}, bf16[384,512]{1,0:T(8,128)(2,1)S(1)}, u32[]{:S(2)}, u32[]{:S(2)}) collective-permute-start(bf16[384,512]{1,0:T(8,128)(2,1)} %get-tuple-element.41), channel_id=1, source_target_pairs={{0,2},{1,3},{2,0},{3,1},{4,6},{5,7},{6,4},{7,5},{8,10},{9,11},{10,... | collective-permute-start | bytes 1179656 | tf_op jit(solution)/shard_map/ppermute | solution.py:22
  185.1 7.8 %copy-start.3 = (bf16[128,4096]{1,0:T(8,128)(2,1)}, bf16[128,4096]{1,0:T(8,128)(2,1)S(1)}, u32[]{:S(2)}) copy-start(bf16[128,4096]{1,0:T(8,128)(2,1)S(1)} %collective-permute-done.14.refs_4_.refs_5_) | copy-start | bytes 3145732
  191.2 1.7 copy-start.4
  192.8 0.7 copy-start.13
  203.7 7.1 %copy-start.16 = (f32[512]{0:T(512)S(1)}, f32[512]{0:T(512)}, u32[]{:S(2)}) copy-start(f32[512]{0:T(512)} %param.22) | copy-start | bytes 6148
  203.8 7.1 %copy-start.17 = (f32[512]{0:T(512)S(1)}, f32[512]{0:T(512)}, u32[]{:S(2)}) copy-start(f32[512]{0:T(512)} %param.21) | copy-start | bytes 6148
  203.8 56.4 %all-to-all-start.1 = ((bf16[32,24,2048]{2,1,0:T(8,128)(2,1)}), bf16[32,24,2048]{2,1,0:T(8,128)(2,1)}, u32[]{:S(2)}, u32[]{:S(2)}) async-start(bf16[32,24,2048]{2,1,0:T(8,128)(2,1)} %bitcast.52), calls=%async_computation.1 | async-start | bytes 6291456 | tf_op jit(solution)/shard_map/all_to_all | solution.py:436
  212.1 11.6 %copy-start.5 = (bf16[256,2048]{1,0:T(8,128)(2,1)S(1)}, bf16[256,2048]{1,0:T(8,128)(2,1)}, u32[]{:S(2)}) copy-start(bf16[256,2048]{1,0:T(8,128)(2,1)} %get-tuple-element.42.refs_0_) | copy-start | bytes 3145732
  218.7 7.3 %copy-start.6 = (bf16[256,2048]{1,0:T(8,128)(2,1)S(1)}, bf16[256,2048]{1,0:T(8,128)(2,1)}, u32[]{:S(2)}) copy-start(bf16[256,2048]{1,0:T(8,128)(2,1)} %get-tuple-element.44.refs_3_) | copy-start | bytes 3145732
  218.7 26.4 %copy-start.8 = (bf16[256,2048]{1,0:T(8,128)(2,1)S(1)}, bf16[256,2048]{1,0:T(8,128)(2,1)}, u32[]{:S(2)}) copy-start(bf16[256,2048]{1,0:T(8,128)(2,1)} %get-tuple-element.34) | copy-start | bytes 3145732
  218.7 26.3 %collective-permute-start.5 = (bf16[256,2048]{1,0:T(8,128)(2,1)}, bf16[256,2048]{1,0:T(8,128)(2,1)}, u32[]{:S(2)}, u32[]{:S(2)}) collective-permute-start(bf16[256,2048]{1,0:T(8,128)(2,1)} %get-tuple-element.35), channel_id=1, source_target_pairs={{0,1},{1,0},{2,3},{3,2},{4,5},{5,4},{6,7},{7,6},{8,9},{9,8},{10,11... | collective-permute-start | bytes 3145736 | tf_op jit(solution)/shard_map/ppermute | solution.py:22
  221.4 28.2 %collective-permute-start.6 = (bf16[256,2048]{1,0:T(8,128)(2,1)}, bf16[256,2048]{1,0:T(8,128)(2,1)S(1)}, u32[]{:S(2)}, u32[]{:S(2)}) collective-permute-start(bf16[256,2048]{1,0:T(8,128)(2,1)} %get-tuple-element.37), channel_id=1, source_target_pairs={{0,3},{1,2},{2,1},{3,0},{4,7},{5,6},{6,5},{7,4},{8,11},{9,10},{10,... | collective-permute-start | bytes 3145736 | tf_op jit(solution)/shard_map/ppermute | solution.py:22
  224.9 35.3 %collective-permute-start.17 = (bf16[128,2048]{1,0:T(8,128)(2,1)S(1)}, bf16[128,2048]{1,0:T(8,128)(2,1)S(1)}, u32[]{:S(2)}, u32[]{:S(2)}) collective-permute-start(bf16[128,2048]{1,0:T(8,128)(2,1)S(1)} %add_convert_fusion.2), channel_id=1, source_target_pairs={{0,3},{1,2},{2,1},{3,0},{4,7},{5,6},{6,5},{7,4},{8,11},{9,10},{10,... | collective-permute-start | bytes 1572872 | tf_op jit(solution)/shard_map/ppermute | solution.py:22
  227.1 22.5 %copy-start.7 = (bf16[256,2048]{1,0:T(8,128)(2,1)S(1)}, bf16[256,2048]{1,0:T(8,128)(2,1)}, u32[]{:S(2)}) copy-start(bf16[256,2048]{1,0:T(8,128)(2,1)} %get-tuple-element.36) | copy-start | bytes 3145732
  227.1 33.0 %collective-permute-start.19 = (bf16[128,2048]{1,0:T(8,128)(2,1)S(1)}, bf16[128,2048]{1,0:T(8,128)(2,1)S(1)}, u32[]{:S(2)}, u32[]{:S(2)}) collective-permute-start(bf16[128,2048]{1,0:T(8,128)(2,1)S(1)} %add_convert_fusion.1), channel_id=1, source_target_pairs={{0,1},{1,0},{2,3},{3,2},{4,5},{5,4},{6,7},{7,6},{8,9},{9,8},{10,11... | collective-permute-start | bytes 1572872 | tf_op jit(solution)/shard_map/ppermute | solution.py:22
  247.4 23.0 %collective-permute-start.7 = (bf16[128,2048]{1,0:T(8,128)(2,1)}, bf16[128,2048]{1,0:T(8,128)(2,1)}, u32[]{:S(2)}, u32[]{:S(2)}) collective-permute-start(bf16[128,2048]{1,0:T(8,128)(2,1)} %get-tuple-element.59), channel_id=1, source_target_pairs={{0,3},{1,2},{2,1},{3,0},{4,7},{5,6},{6,5},{7,4},{8,11},{9,10},{10,... | collective-permute-start | bytes 1572872 | tf_op jit(solution)/shard_map/ppermute | solution.py:22
  250.8 19.6 %collective-permute-start.8 = (bf16[128,2048]{1,0:T(8,128)(2,1)}, bf16[128,2048]{1,0:T(8,128)(2,1)}, u32[]{:S(2)}, u32[]{:S(2)}) collective-permute-start(bf16[128,2048]{1,0:T(8,128)(2,1)} %get-tuple-element.57), channel_id=1, source_target_pairs={{0,1},{1,0},{2,3},{3,2},{4,5},{5,4},{6,7},{7,6},{8,9},{9,8},{10,11... | collective-permute-start | bytes 1572872 | tf_op jit(solution)/shard_map/ppermute | solution.py:22
  260.1 0.8 copy-start.11
  260.1 1.0 copy-start.12
  261.1 12.3 %copy-start.1 = (bf16[4096,256]{1,0:T(8,128)(2,1)S(1)}, bf16[4096,256]{1,0:T(8,128)(2,1)}, u32[]{:S(2)}) copy-start(bf16[4096,256]{1,0:T(8,128)(2,1)} %param.31) | copy-start | bytes 6291460
